TPU v7x, 32 devices: a whole 2x2x4 slice. The times are simulated.
32 devices in a mesh: ep: 8 (over z, x), tp: 4 (over y, core).
Axes of the slice: x: 2, y: 2, z: 4, core: 2. Of those that a mesh axis runs over, the one named last changes fastest.
Arguments:
- mixer_group_input: bfloat16 [2048, 1024], P('ep', 'tp'), may hold values from -6 to 6
- log_step_size: float32 [64, 2048], P('tp', 'ep'), may hold values from -16 to 0
- extra_log_decay: float32 [64, 2048], P('tp', 'ep'), may hold values from -0.7 to 0
- negated_eigen_real: float32 [64, 64], P('tp'), may hold values from 0.35 to 0.7
- frequency: float32 [64, 64], P('tp'), may hold values from 0 to 200
- group_input_matrices: bfloat16 [2, 64, 64, 16], P(None, 'tp'), may hold values from -1.5 to 1.5
- group_output_matrices: bfloat16 [2, 64, 16, 64], P(None, 'tp'), may hold values from -0.5 to 0.5
- channel_feedthrough: float32 [1024], P('tp'), may hold values from -3 to 3
- mixer_norm_scale: float32 [1024], replicated, may hold values from 0.1 to 1.9
- mixer_output_weight: bfloat16 [1024, 2048], P(None, 'tp'), may hold values from -0.1875 to 0.1875
- second_micro_input: bfloat16 [1024, 2048], P('ep'), may hold values from -6 to 6
- expert_norm_scale: float32 [2048], replicated, may hold values from 0.1 to 1.9
- routes: int32 [1024, 4], P('ep'), may hold values from 0 to 7, all different within a row; in each aligned block of 128 rows (0 to 127, 128 to 255, ...) at most 128 rows name the same one
- chosen_expert_weight: float32 [1024, 4], P('ep'), may hold values from 0.1 to 1
- expert_gate_weight: bfloat16 [8, 2048, 2048], P('ep', None, 'tp'), may hold values from -0.125 to 0.125
- expert_up_weight: bfloat16 [8, 2048, 2048], P('ep', None, 'tp'), may hold values from -0.125 to 0.125
- expert_down_weight: bfloat16 [8, 2048, 2048], P('ep', None, 'tp'), may hold values from -0.125 to 0.125
- shared_gate_weight: bfloat16 [2048, 2048], P(None, 'tp'), may hold values from -0.125 to 0.125
- shared_up_weight: bfloat16 [2048, 2048], P(None, 'tp'), may hold values from -0.125 to 0.125
- shared_down_weight: bfloat16 [2048, 2048], P(None, 'tp'), may hold values from -0.125 to 0.125
Outputs:
- mixed: bfloat16 [2048, 2048], P('ep', 'tp')
- moe_out: bfloat16 [1024, 2048], P('ep', 'tp')
Inputs may be any that keep to these rules, and one draw needn't show every extreme that they name: `routes`: each row names 4 different experts; in each aligned block of 128 rows no expert is named by more than 128 rows, and in some block one expert is named by exactly 128 rows.
All inputs are finite; a program needn't handle non-finite values.
Results may differ from a plain program's by a relative error of at most 0.0068.
Values may be sent and summed in bfloat16 or wider, within the bound.
A program may use at most 192 MiB of HBM per device.

v0:
```python
import jax
import jax.numpy as jnp
from jax import lax
from jax.experimental import pallas as pl
from jax.experimental.pallas import tpu as pltpu
from jax.sharding import PartitionSpec as P

eps_norm = 1e-06
LANES = 128
ROWS = 8


def cos_sin(angle):
    turns = jnp.floor(angle * 0.6366197723675814 + 0.5)
    rest = ((angle - turns * 1.5703125) - turns * 4.837512969970703125e-4) - turns * 7.549789954891882e-8
    square = rest * rest
    sine = rest + rest * square * (
        -1.6666654611e-1 + square * (8.3321608736e-3 + square * -1.9515295891e-4)
    )
    cosine = (
        1.0
        - 0.5 * square
        + square
        * square
        * (
            4.166664568298827e-2
            + square * (-1.388731625493765e-3 + square * 2.443315711809948e-5)
        )
    )
    quarter = turns.astype(jnp.int32)
    odd = (quarter & 1) == 1
    out_cos = jnp.where(odd, sine, cosine)
    out_sin = jnp.where(odd, cosine, sine)
    out_cos = jnp.where(((quarter + 1) & 2) == 2, -out_cos, out_cos)
    out_sin = jnp.where((quarter & 2) == 2, -out_sin, out_sin)
    return out_cos, out_sin


def one_minus_exp_neg(y):
    series = y * (
        1.0
        - y / 2
        * (1.0 - y / 3 * (1.0 - y / 4 * (1.0 - y / 5 * (1.0 - y / 6))))
    )
    return jnp.where(y < 0.3, series, 1.0 - jnp.exp(-y))


def scan_kernel(
    u_ref, win_ref, step_ref, loss_ref, eig_ref, freq_ref,
    reach_r_ref, reach_i_ref, state_r_ref, state_i_ref, ends_ref,
    ar_ref, ai_ref, br_ref, bi_ref,
):
    rows = u_ref.shape[0]
    u = u_ref[...]
    lane = lax.broadcasted_iota(jnp.int32, (rows, LANES), 1)
    half = lane < (LANES // step_ref.shape[2])
    step = jnp.where(half, step_ref[0, :, 0:1], step_ref[0, :, 1:2])
    loss = jnp.where(half, loss_ref[0, :, 0:1], loss_ref[0, :, 1:2])
    loss_rate = eig_ref[0] * step
    magnitude = jnp.exp(loss - loss_rate)
    cosine, sine = cos_sin(freq_ref[0] * step)
    scaling = jnp.sqrt(one_minus_exp_neg(2.0 * loss_rate))
    ar_ref[...] = magnitude * cosine
    ai_ref[...] = magnitude * sine
    br_ref[...] = scaling * jnp.dot(u, win_ref[0], preferred_element_type=jnp.float32)
    bi_ref[...] = scaling * jnp.dot(u, win_ref[1], preferred_element_type=jnp.float32)
    count = rows // ROWS
    reach = jnp.ones((ROWS, LANES), jnp.float32), jnp.zeros((ROWS, LANES), jnp.float32)
    state = jnp.zeros((ROWS, LANES), jnp.float32), jnp.zeros((ROWS, LANES), jnp.float32)
    for j in range(count):
        at = pl.ds(j * ROWS, ROWS)
        ar, ai, br, bi = ar_ref[at, :], ai_ref[at, :], br_ref[at, :], bi_ref[at, :]
        reach = ar * reach[0] - ai * reach[1], ar * reach[1] + ai * reach[0]
        state = ar * state[0] - ai * state[1] + br, ar * state[1] + ai * state[0] + bi
        ar_ref[at, :] = reach[0]
        ai_ref[at, :] = reach[1]
        br_ref[at, :] = state[0]
        bi_ref[at, :] = state[1]
    row = lax.broadcasted_iota(jnp.int32, (ROWS, LANES), 0)
    er, ei = jnp.ones((1, LANES), jnp.float32), jnp.zeros((1, LANES), jnp.float32)
    sr, si = jnp.zeros((1, LANES), jnp.float32), jnp.zeros((1, LANES), jnp.float32)
    pre_r, pre_i = reach[0] * 0.0, reach[0] * 0.0
    pre_sr, pre_si = pre_r, pre_r
    for s in range(ROWS):
        here = row == s
        pre_r = jnp.where(here, er, pre_r)
        pre_i = jnp.where(here, ei, pre_i)
        pre_sr = jnp.where(here, sr, pre_sr)
        pre_si = jnp.where(here, si, pre_si)
        tr, ti = reach[0][s : s + 1], reach[1][s : s + 1]
        ur, ui = state[0][s : s + 1], state[1][s : s + 1]
        er, ei, sr, si = (
            tr * er - ti * ei,
            tr * ei + ti * er,
            tr * sr - ti * si + ur,
            tr * si + ti * sr + ui,
        )
    for j in range(count):
        at = pl.ds(j * ROWS, ROWS)
        ar, ai = ar_ref[at, :], ai_ref[at, :]
        state_r_ref[at, :] = br_ref[at, :] + ar * pre_sr - ai * pre_si
        state_i_ref[at, :] = bi_ref[at, :] + ar * pre_si + ai * pre_sr
        reach_r_ref[at, :] = ar * pre_r - ai * pre_i
        reach_i_ref[at, :] = ar * pre_i + ai * pre_r
    ends_ref[0, 0:1] = er
    ends_ref[0, 1:2] = ei
    ends_ref[0, 2:3] = sr
    ends_ref[0, 3:4] = si


def read_kernel(
    hops, ends_ref, reach_r_ref, reach_i_ref, state_r_ref, state_i_ref, wout_ref, u_ref, feed_ref,
    out_ref, total_ref,
):
    tile = pl.program_id(0)
    place = jnp.full((1, LANES), lax.axis_index("ep"), jnp.int32)
    sr, si = jnp.zeros((1, LANES), jnp.float32), jnp.zeros((1, LANES), jnp.float32)
    for hop in range(hops - 1):
        keep = place > hop
        tr, ti = ends_ref[hop, 0, 0:1], ends_ref[hop, 0, 1:2]
        ur, ui = ends_ref[hop, 0, 2:3], ends_ref[hop, 0, 3:4]
        sr, si = (
            jnp.where(keep, tr * sr - ti * si + ur, sr),
            jnp.where(keep, tr * si + ti * sr + ui, si),
        )
    reach_r, reach_i = reach_r_ref[...], reach_i_ref[...]
    state_r = state_r_ref[...] + reach_r * sr - reach_i * si
    state_i = state_i_ref[...] + reach_r * si + reach_i * sr

    def product(state, weight):
        high = state.astype(jnp.bfloat16)
        low = (state - high.astype(jnp.float32)).astype(jnp.bfloat16)
        return jnp.dot(high, weight, preferred_element_type=jnp.float32) + jnp.dot(
            low, weight, preferred_element_type=jnp.float32
        )

    part = product(state_r, wout_ref[0]) - product(state_i, wout_ref[1])

    @pl.when(tile == 0)
    def _():
        total_ref[...] = part + feed_ref[...] * u_ref[...].astype(jnp.float32)

    @pl.when(tile > 0)
    def _():
        total_ref[...] += part

    @pl.when(tile == pl.num_programs(0) - 1)
    def _():
        value = total_ref[...]
        inner = 0.7978845608028654 * (value + 0.044715 * (value * value * value))
        out_ref[...] = (0.5 * value * (1.0 + jnp.tanh(inner))).astype(out_ref.dtype)


def mixer_local(
    inputs, step_logs, losses, eigen, frequency, group_in, group_out, feedthrough
):
    positions, channels = inputs.shape
    groups, states = eigen.shape
    width = groups * states
    tiles = width // LANES
    per_tile = groups // tiles
    seg = positions // ROWS

    def shuffled(rows):
        return rows.reshape(ROWS, seg, -1).transpose(1, 0, 2).reshape(positions, -1)

    def by_tile(table):
        wide = shuffled(table.T).reshape(positions, tiles, per_tile)
        return wide.transpose(1, 0, 2)

    u = shuffled(inputs)
    same = jnp.eye(groups, dtype=bool)
    zero = jnp.zeros((), group_in.dtype)
    win = jnp.where(
        same[None, :, None, :, None], group_in.transpose(0, 1, 3, 2)[:, :, :, None, :], zero
    ).reshape(2, channels, width)
    wout = jnp.where(
        same[None, :, None, :, None], group_out.transpose(0, 1, 3, 2)[:, :, :, None, :], zero
    ).reshape(2, width, channels)
    column = pl.BlockSpec((positions, LANES), lambda i: (0, i))
    whole_u = pl.BlockSpec((positions, channels), lambda i: (0, 0))
    pair = pl.BlockSpec((1, positions, per_tile), lambda i: (i, 0, 0))
    lane_row = pl.BlockSpec((1, 1, LANES), lambda i: (i, 0, 0))
    wide_shape = jax.ShapeDtypeStruct((positions, width), jnp.float32)
    column_scratch = pltpu.VMEM((positions, LANES), jnp.float32)
    reach_r, reach_i, state_r, state_i, ends = pl.pallas_call(
        scan_kernel,
        grid=(tiles,),
        in_specs=[
            whole_u,
            pl.BlockSpec((2, channels, LANES), lambda i: (0, 0, i)),
            pair,
            pair,
            lane_row,
            lane_row,
        ],
        out_specs=[column, column, column, column, pl.BlockSpec((1, 4, LANES), lambda i: (i, 0, 0))],
        out_shape=[wide_shape] * 4 + [jax.ShapeDtypeStruct((tiles, 4, LANES), jnp.float32)],
        scratch_shapes=[column_scratch] * 4,
        cost_estimate=pl.CostEstimate(
            flops=positions * channels * width * 4, bytes_accessed=24 * positions * width,
            transcendentals=4 * positions * width,
        ),
        name="scan_states",
    )(
        u,
        win,
        by_tile(jnp.exp(step_logs)),
        by_tile(losses),
        eigen.reshape(tiles, 1, LANES),
        frequency.reshape(tiles, 1, LANES),
    )
    hops = lax.axis_size("ep")
    all_ends = lax.all_gather(ends, "ep")
    out = pl.pallas_call(
        lambda *refs: read_kernel(hops, *refs),
        grid=(tiles,),
        in_specs=[
            pl.BlockSpec((hops, 1, 4, LANES), lambda i: (0, i, 0, 0)),
            column, column, column, column,
            pl.BlockSpec((2, LANES, channels), lambda i: (0, i, 0)),
            whole_u,
            pl.BlockSpec((1, channels), lambda i: (0, 0)),
        ],
        out_specs=whole_u,
        out_shape=jax.ShapeDtypeStruct((positions, channels), jnp.bfloat16),
        scratch_shapes=[pltpu.VMEM((positions, channels), jnp.float32)],
        cost_estimate=pl.CostEstimate(
            flops=positions * channels * width * 8, bytes_accessed=24 * positions * width,
            transcendentals=positions * channels,
        ),
        name="read_states",
    )(all_ends, reach_r, reach_i, state_r, state_i, wout, u, feedthrough.reshape(1, channels))
    return out.reshape(seg, ROWS, channels).transpose(1, 0, 2).reshape(positions, channels)


def scaled_rows(values, gain):
    widened = values.astype(jnp.float32)
    factor = lax.rsqrt(jnp.mean(widened * widened, axis=-1, keepdims=True) + eps_norm)
    return (widened * factor * gain).astype(jnp.bfloat16)


def gated(rows, gate_weight, up_weight):
    gate_part = jnp.dot(rows, gate_weight, preferred_element_type=jnp.float32)
    up_part = jnp.dot(rows, up_weight, preferred_element_type=jnp.float32)
    return (jax.nn.silu(gate_part) * up_part).astype(jnp.bfloat16)


def on_device(
    mixer_group_input,
    log_step_size,
    extra_log_decay,
    negated_eigen_real,
    frequency,
    group_input_matrices,
    group_output_matrices,
    channel_feedthrough,
    mixer_norm_scale,
    mixer_output_weight,
    second_micro_input,
    expert_norm_scale,
    routes,
    chosen_expert_weight,
    expert_gate_weight,
    expert_up_weight,
    expert_down_weight,
    shared_gate_weight,
    shared_up_weight,
    shared_down_weight,
):
    token_count, top_count = routes.shape
    experts = lax.axis_size("ep")
    column_count = expert_down_weight.shape[2]
    gate_weight, up_weight, down_weight = (
        expert_gate_weight[0],
        expert_up_weight[0],
        expert_down_weight[0],
    )
    normed_tokens = scaled_rows(second_micro_input, expert_norm_scale)
    model_width = normed_tokens.shape[1]
    part = lax.rem(lax.axis_index("tp"), 2)
    own_half = lax.dynamic_slice_in_dim(
        normed_tokens, part * (model_width // 2), model_width // 2, 1
    )
    half_tokens = lax.all_gather(own_half, "ep", axis=0, tiled=True)
    pairs = [[2 * i, 2 * i + 1] for i in range(lax.axis_size("tp") // 2)]
    all_tokens = lax.all_gather(
        half_tokens, "tp", axis=1, tiled=True, axis_index_groups=pairs
    )
    ssm_out = mixer_local(
        mixer_group_input,
        log_step_size,
        extra_log_decay,
        negated_eigen_real,
        frequency,
        group_input_matrices,
        group_output_matrices,
        channel_feedthrough,
    )
    shared_hidden = gated(normed_tokens, shared_gate_weight, shared_up_weight)
    whole_rows = lax.all_gather(ssm_out, "tp", axis=1, tiled=True)
    whole_shared = lax.all_gather(shared_hidden, "tp", axis=1, tiled=True)
    hidden = gated(all_tokens, gate_weight, up_weight)
    whole_hidden = lax.all_gather(hidden, "tp", axis=1, tiled=True)
    normed_mix = scaled_rows(whole_rows, mixer_norm_scale)
    mixed = jnp.dot(normed_mix, mixer_output_weight, preferred_element_type=jnp.float32).astype(
        jnp.bfloat16
    )
    shared_columns = jnp.dot(
        whole_shared, shared_down_weight, preferred_element_type=jnp.float32
    )
    results = (
        jnp.dot(whole_hidden, down_weight, preferred_element_type=jnp.float32)
        .astype(jnp.bfloat16)
        .reshape(experts, token_count, column_count)
    )
    returned = lax.all_to_all(results, "ep", split_axis=0, concat_axis=0, tiled=True)
    share = jnp.sum(
        jnp.where(
            routes[:, :, None] == jnp.arange(experts, dtype=jnp.int32),
            chosen_expert_weight[:, :, None],
            0.0,
        ),
        axis=1,
    )
    combined = jnp.sum(returned.astype(jnp.float32) * share.T[:, :, None], axis=0)
    moe_out = (shared_columns + combined).astype(jnp.bfloat16)
    return (mixed, moe_out)


def solution(mesh):
    return jax.shard_map(
        on_device,
        mesh=mesh,
        in_specs=(
            P("ep", "tp"),
            P("tp", "ep"),
            P("tp", "ep"),
            P("tp", None),
            P("tp", None),
            P(None, "tp", None, None),
            P(None, "tp", None, None),
            P("tp"),
            P(),
            P(None, "tp"),
            P("ep", None),
            P(),
            P("ep", None),
            P("ep", None),
            P("ep", None, "tp"),
            P("ep", None, "tp"),
            P("ep", None, "tp"),
            P(None, "tp"),
            P(None, "tp"),
            P(None, "tp"),
        ),
        out_specs=(P("ep", "tp"), P("ep", "tp")),
        check_vma=False,
    )
```

profile of v0, /device:TPU:0, one launch (start us, length us, event | category | flops | bytes accessed | tf_op | source)
XLA Modules:
  0.0 227.0 jit_solution(16338142779001281035)
XLA Ops:
  7.2 1.4 fusion.16
  8.6 1.2 fusion.18
  9.9 0.8 copy-done.2
  10.7 0.7 constant_dynamic-slice_fusion
  11.5 51.9 %all-gather.5.cloned.1.call-done = bf16[1024,1024]{1,0:T(8,128)(2,1)} async-done(((bf16[128,1024]{1,0:T(8,128)(2,1)}), bf16[1024,1024]{1,0:T(8,128)(2,1)}) %all-gather.5.cloned.1.call-update) | async-done | bytes 2097168 | tf_op jit(solution)/shard_map/all_gather | solution.py:285
  63.5 13.7 %all-gather.7.cloned.1.call-done = bf16[1024,2048]{1,0:T(8,128)(2,1)} async-done(((bf16[1024,1024]{1,0:T(8,128)(2,1)}), bf16[1024,2048]{1,0:T(8,128)(2,1)}) %all-gather.7.cloned.1.call-update) | async-done | bytes 4194320 | tf_op jit(solution)/shard_map/all_gather | solution.py:287
  77.2 4.7 %fusion.2 = f32[1024,512]{1,0:T(8,128)S(1)} fusion(bf16[1024,2048]{1,0:T(8,128)(2,1)} %all-gather.7.cloned.1.call-done, bf16[1,2048,512]{2,1,0:T(8,128)(2,1)S(1)} %copy-done), kind=kOutput, calls=%fused_computation.2 | convolution fusion | flops 2147483648 | bytes 8388608 | tf_op jit(solution)/shard_map/dot_general | solution.py:245
  81.8 3.6 %multiply_convert_fusion = bf16[1024,512]{1,0:T(8,128)(2,1)} fusion(f32[1024,512]{1,0:T(8,128)S(1)} %fusion.2, bf16[1024,2048]{1,0:T(8,128)(2,1)S(1)} %copy-done.13, bf16[1,2048,512]{2,1,0:T(8,128)(2,1)S(1)} %copy-done.14), kind=kOutput, calls=%fused_computation.7 | convolution fusion | flops 2150629376 | bytes 9437184 | tf_op jit(solution)/shard_map/dot_general | solution.py:244
  85.5 0.6 copy-done.8
  86.1 0.1 copy.51
  86.2 0.2 broadcast_in_dim.76
  86.4 0.8 broadcast_in_dim.77
  87.2 1.7 broadcast_in_dim.79
  88.9 3.3 %broadcast_in_dim.80 = bf16[2,256,1024]{2,1,0:T(8,128)(2,1)S(1)} reshape(bf16[2,16,16,16,64]{4,3,2,1,0:T(8,128)(2,1)} %broadcast_in_dim.79) | data formatting | bytes 2097152 | tf_op jit(solution)/shard_map/jit(_where)/broadcast_in_dim | solution.py:174
  92.2 0.7 copy.61
  92.9 0.7 exponential_bitcast_fusion
  93.6 0.1 reshape.72
  93.7 0.8 copy.52
  94.6 1.1 reshape_reshape.6
  95.7 1.4 copy.53
  97.1 0.1 reshape.73
  97.2 0.8 copy.54
  98.0 1.1 reshape_reshape.7
  99.1 1.4 copy.55
  100.6 1.4 reshape.74.eig_ref
  101.9 1.4 reshape.75.freq_ref
  103.3 1.7 broadcast_in_dim.82
  105.0 2.5 %broadcast_in_dim.83 = pred[1024,256]{0,1:T(8,128)(4,1)} reshape(pred[16,64,16,16]{1,0,3,2:T(8,128)(4,1)} %broadcast_in_dim.82) | data formatting | bytes 524288 | tf_op jit(solution)/shard_map/jit(_where)/broadcast_in_dim | solution.py:177
  107.5 2.0 copy.56
  109.5 1.8 broadcast_in_dim.85
  111.3 4.1 %broadcast_in_dim.86 = bf16[2,1024,256]{1,2,0:T(8,128)(2,1)} reshape(bf16[2,16,64,16,16]{2,1,4,3,0:T(8,128)(2,1)} %broadcast_in_dim.85) | data formatting | bytes 2097152 | tf_op jit(solution)/shard_map/jit(_where)/broadcast_in_dim | solution.py:177
  115.4 2.3 %copy.58 = bf16[2,1024,256]{2,1,0:T(8,128)(2,1)} copy(bf16[2,1024,256]{1,2,0:T(8,128)(2,1)} %broadcast_in_dim.86) | data formatting | bytes 2097152 | tf_op jit(solution)/shard_map/jit(_where)/broadcast_in_dim | solution.py:177
  117.7 1.2 broadcast_select_fusion.1.win_ref
  118.9 9.2 %scan_states.1 = (f32[256,1024]{1,0:T(8,128)}, f32[256,1024]{1,0:T(8,128)}, f32[256,1024]{1,0:T(8,128)}, f32[256,1024]{1,0:T(8,128)}, f32[8,4,128]{2,1,0:T(4,128)}) custom-call(bf16[256,256]{1,0:T(8,128)(2,1)} %bitcast.68, bf16[2,256,1024]{2,1,0:T(8,128)(2,1)} %broadcast_select_fusion.1.win_ref, f32[8,256,2]{2,1,0:T(8,128)} %bitcast.66, ...), custom_call_target="tpu_custom_call" | custom-call | flops 268435456 | bytes 6291456 | tf_op jit(solution)/shard_map/scan_states/pallas_call | solution.py:186
  128.1 1.2 broadcast_select_fusion.refs_5_
  129.3 6.2 %fusion.8 = bf16[1024,512]{1,0:T(8,128)(2,1)} fusion(bf16[1024,2048]{1,0:T(8,128)(2,1)} %all-gather.9.cloned.1.call-done, bf16[1,2048,512]{2,1,0:T(8,128)(2,1)} %param.36), kind=kOutput, calls=%fused_computation.8 | convolution fusion | flops 2148007936 | bytes 7340032 | tf_op jit(solution)/shard_map/dot_general | solution.py:313
  135.5 6.0 %all-to-all-start = ((bf16[8,128,512]{2,1,0:T(8,128)(2,1)}), bf16[8,128,512]{2,1,0:T(8,128)(2,1)S(1)}, u32[]{:S(2)}, u32[]{:S(2)}) async-start(bf16[8,128,512]{2,1,0:T(8,128)(2,1)} %bitcast.72), calls=%async_computation | async-start | bytes 2097152 | tf_op jit(solution)/shard_map/all_to_all | solution.py:317
  141.4 48.4 %all-gather = f32[64,4,128]{2,1,0:T(4,128)} all-gather(f32[8,4,128]{2,1,0:T(4,128)S(1)} %copy-done.10), channel_id=2, replica_groups=mesh['ep'=8,'tp'=4] {'ep'}, dimensions={0}, use_global_device_ids=true | all-gather | bytes 147456 | tf_op jit(solution)/shard_map/all_gather | solution.py:214
  189.8 7.4 %read_states.1 = bf16[256,256]{1,0:T(8,128)(2,1)} custom-call(f32[8,8,4,128]{3,2,1,0:T(4,128)} %bitcast.73, f32[256,1024]{1,0:T(8,128)} %get-tuple-element.8.refs_1_, f32[256,1024]{1,0:T(8,128)} %get-tuple-element.9.refs_2_, f32[256,1024]{1,0:T(8,128)} %get-tuple-element.10.refs_3_, f32[256,1024]{1,0:T(8,128)} %get-tuple-element.11.refs_4_, ...), custom_call_target="tpu_custom_call" | custom-call | flops 536870912 | bytes 6291456 | tf_op jit(solution)/shard_map/read_states/pallas_call | solution.py:215
  197.2 0.9 copy.59
  198.2 7.3 %all_gather.23 = bf16[256,1024]{1,0:T(8,128)(2,1)S(1)} all-gather(bf16[256,256]{1,0:T(8,128)(2,1)S(1)} %bitcast.75), channel_id=1, replica_groups=mesh['ep'=8,'tp'=4] {'tp'}, dimensions={1}, use_global_device_ids=true | all-gather | bytes 655360 | tf_op jit(solution)/shard_map/all_gather | solution.py:301
  205.5 0.2 fusion.13
  205.7 2.2 fusion.22
  207.9 0.5 fusion.11
  208.4 7.7 %all_gather.24 = bf16[128,2048]{1,0:T(8,128)(2,1)} all-gather(bf16[128,512]{1,0:T(8,128)(2,1)S(1)} %fusion.11), channel_id=1, replica_groups=mesh['ep'=8,'tp'=4] {'tp'}, dimensions={1}, use_global_device_ids=true | all-gather | bytes 655360 | tf_op jit(solution)/shard_map/all_gather | solution.py:302
  216.2 1.2 convolution_convert_fusion
  217.4 0.3 multiply_reduce_fusion
  217.6 2.9 %fusion.12 = bf16[128,512]{1,0:T(8,128)(2,1)} fusion(f32[128,512]{1,0:T(8,128)S(1)} %multiply_reduce_fusion, bf16[128,2048]{1,0:T(8,128)(2,1)} %all_gather.24, bf16[2048,512]{1,0:T(8,128)(2,1)} %param.39), kind=kOutput, calls=%fused_computation.17 | convolution fusion | flops 268566528 | bytes 3014656 | tf_op jit(solution)/shard_map/dot_general | solution.py:309
  (47 shorter events, 0.3 us)
Async XLA Ops:
  7.2 70.0 %copy-start = (bf16[1,2048,512]{2,1,0:T(8,128)(2,1)S(1)}, bf16[1,2048,512]{2,1,0:T(8,128)(2,1)}, u32[]{:S(2)}) copy-start(bf16[1,2048,512]{2,1,0:T(8,128)(2,1)} %param.35) | copy-start | bytes 6291460
  7.2 56.2 %all-gather.5.cloned.1.call-start = ((), (), s32[]{:S(2)}) async-start(), calls=%async_computation.1 | async-start | bytes 2359296 | tf_op jit(solution)/shard_map/all_gather | solution.py:285
  9.8 0.8 copy-start.2
  11.4 65.7 %all-gather.7.cloned.1.call-start = ((), (), s32[]{:S(2)}) async-start(), calls=%async_computation.2 | async-start | bytes 6291456 | tf_op jit(solution)/shard_map/all_gather | solution.py:287
  63.4 65.9 %all-gather.9.cloned.1.call-start = ((), (), s32[]{:S(2)}) async-start(), calls=%async_computation.3 | async-start | bytes 5242880 | tf_op jit(solution)/shard_map/all_gather | solution.py:304
  77.2 4.7 %copy-start.13 = (bf16[1024,2048]{1,0:T(8,128)(2,1)S(1)}, bf16[1024,2048]{1,0:T(8,128)(2,1)}, u32[]{:S(2)}) copy-start(bf16[1024,2048]{1,0:T(8,128)(2,1)} %all-gather.7.cloned.1.call-done) | copy-start | bytes 12582916
  77.2 4.7 %copy-start.14 = (bf16[1,2048,512]{2,1,0:T(8,128)(2,1)S(1)}, bf16[1,2048,512]{2,1,0:T(8,128)(2,1)}, u32[]{:S(2)}) copy-start(bf16[1,2048,512]{2,1,0:T(8,128)(2,1)} %param.34) | copy-start | bytes 6291460
  85.5 1.7 copy-start.5
  85.5 0.6 copy-start.8
  88.9 3.3 %copy-start.6 = (bf16[256,256]{1,0:T(8,128)(2,1)S(1)}, bf16[256,256]{1,0:T(8,128)(2,1)}, u32[]{:S(2)}) copy-start(bf16[256,256]{1,0:T(8,128)(2,1)} %param.20) | copy-start | bytes 393220
  88.9 8.2 %copy-start.9 = (f32[16,256]{1,0:T(8,128)S(1)}, f32[16,256]{1,0:T(8,128)}, u32[]{:S(2)}) copy-start(f32[16,256]{1,0:T(8,128)} %param.22) | copy-start | bytes 49156
  98.0 11.4 %copy-start.7 = (bf16[2,16,16,64]{3,2,1,0:T(8,128)(2,1)S(1)}, bf16[2,16,16,64]{3,2,1,0:T(8,128)(2,1)}, u32[]{:S(2)}) copy-start(bf16[2,16,16,64]{3,2,1,0:T(8,128)(2,1)} %param.26) | copy-start | bytes 196612
  118.9 9.2 %copy-start.1 = (bf16[2,1024,256]{2,1,0:T(8,128)(2,1)S(1)}, bf16[2,1024,256]{2,1,0:T(8,128)(2,1)}, u32[]{:S(2)}) copy-start(bf16[2,1024,256]{2,1,0:T(8,128)(2,1)} %copy.58) | copy-start | bytes 3145732
  118.9 9.2 %copy-start.4 = (pred[1024,256]{1,0:T(8,128)(4,1)S(1)}, pred[1024,256]{1,0:T(8,128)(4,1)}, u32[]{:S(2)}) copy-start(pred[1024,256]{1,0:T(8,128)(4,1)} %copy.56) | copy-start | bytes 786436
  135.5 6.0 %copy-start.10 = (f32[8,4,128]{2,1,0:T(4,128)S(1)}, f32[8,4,128]{2,1,0:T(4,128)}, u32[]{:S(2)}) copy-start(f32[8,4,128]{2,1,0:T(4,128)} %get-tuple-element.7) | copy-start | bytes 49156
  135.5 81.9 %all-to-all-start = ((bf16[8,128,512]{2,1,0:T(8,128)(2,1)}), bf16[8,128,512]{2,1,0:T(8,128)(2,1)S(1)}, u32[]{:S(2)}, u32[]{:S(2)}) async-start(bf16[8,128,512]{2,1,0:T(8,128)(2,1)} %bitcast.72), calls=%async_computation | async-start | bytes 2097152 | tf_op jit(solution)/shard_map/all_to_all | solution.py:317
  189.8 8.4 %copy-start.11 = (f32[128,4]{0,1:T(4,128)S(1)}, f32[128,4]{0,1:T(4,128)}, u32[]{:S(2)}) copy-start(f32[128,4]{0,1:T(4,128)} %param.33) | copy-start | bytes 6148
  189.8 8.4 %copy-start.12 = (s32[128,4]{0,1:T(4,128)S(1)}, s32[128,4]{0,1:T(4,128)}, u32[]{:S(2)}) copy-start(s32[128,4]{0,1:T(4,128)} %param.32) | copy-start | bytes 6148
  198.2 9.7 %copy-start.3 = (bf16[128,2048]{1,0:T(8,128)(2,1)S(1)}, bf16[128,2048]{1,0:T(8,128)(2,1)}, u32[]{:S(2)}) copy-start(bf16[128,2048]{1,0:T(8,128)(2,1)} %copy-done.2) | copy-start | bytes 1572868
  198.2 9.7 %copy-start.15 = (bf16[2048,512]{1,0:T(8,128)(2,1)S(1)}, bf16[2048,512]{1,0:T(8,128)(2,1)}, u32[]{:S(2)}) copy-start(bf16[2048,512]{1,0:T(8,128)(2,1)} %param.38) | copy-start | bytes 6291460
  207.9 8.2 %copy-start.16 = (bf16[1024,512]{1,0:T(8,128)(2,1)S(1)}, bf16[1024,512]{1,0:T(8,128)(2,1)}, u32[]{:S(2)}) copy-start(bf16[1024,512]{1,0:T(8,128)(2,1)} %param.29) | copy-start | bytes 3145732
  207.9 8.2 %copy-start.17 = (f32[1024]{0:T(1024)S(1)}, f32[1024]{0:T(1024)}, u32[]{:S(2)}) copy-start(f32[1024]{0:T(1024)} %param.28) | copy-start | bytes 12292
Sparse Core Ops, SparseCore 0:
  11.5 51.7 all-gather.4
  64.9 12.1 all-gather.6
  85.6 35.6 all-gather.8
where the time goes:
time: 228 us; the launch traced here: 227 us
  waiting for transfers between devices  65.7 us (29%)
  blocking collectives  63.4 us (28%)
  local copies, waits for them, and re-layouts  34.7 us (15%)
  matrix products  21.2 us (9%)
  Pallas kernels  16.6 us (7%)
  between operations  14 us (6%)
  starting transfers between devices  6.07 us (3%)
  other arithmetic  5.42 us (2%)
    all_gather x1, waiting for transfers between devices, on_device(): half_tokens = lax.all_gather(own_half, 'ep', axis=0, tiled=True)  51.9 us
    all_gather x1, blocking collectives, mixer_local(): all_ends = lax.all_gather(ends, 'ep')  48.4 us
    broadcast_in_dim x6, local copies, waits for them, and re-layouts, mixer_local(): jnp.where(same[None, :, None, :, None], group_out.transpose(0, 1, 3, 2)[:...  14.4 us
    all_gather x1, waiting for transfers between devices, on_device(): lax.all_gather(half_tokens, 'tp', axis=1, tiled=True, axis_index_groups=p...  13.7 us
    pallas_call x1, Pallas kernels, mixer_local(): pl.pallas_call(scan_kernel, grid=(tiles,), in_specs=[whole_u, pl.BlockSpe...  9.21 us
    all_gather x1, blocking collectives, on_device(): whole_shared = lax.all_gather(shared_hidden, 'tp', axis=1, tiled=True)  7.73 us
    pallas_call x1, Pallas kernels, mixer_local(): pl.pallas_call(lambda *refs: read_kernel(hops, *refs), grid=(tiles,), in_...  7.42 us
    all_gather x1, blocking collectives, on_device(): whole_rows = lax.all_gather(ssm_out, 'tp', axis=1, tiled=True)  7.28 us
  transfers between devices with their start and end apart: 4, of which 2 were waited for; matrix products, arithmetic and copies ran while one was open for 17% of the time, Pallas kernels for 7%

commit v1 on v0

v1 whole, which is shorter than its diff:
```python
import functools

import jax
import jax.numpy as jnp
from jax import lax
from jax.experimental import pallas as pl
from jax.experimental.pallas import tpu as pltpu
from jax.sharding import PartitionSpec as P

eps_norm = 1e-06
LANES = 128
ROWS = 8
MESH = pl.DeviceIdType.MESH
bf16, f32 = jnp.bfloat16, jnp.float32
COLUMN_LAG = 1
DOWN_LAG = 2
TILES_PER_STEP = 2
VMEM_BYTES = 62 * 1024 * 1024


def cos_sin(angle):
    turns = jnp.floor(angle * 0.6366197723675814 + 0.5)
    rest = ((angle - turns * 1.5703125) - turns * 4.837512969970703125e-4) - turns * 7.549789954891882e-8
    square = rest * rest
    sine = rest + rest * square * (
        -1.6666654611e-1 + square * (8.3321608736e-3 + square * -1.9515295891e-4)
    )
    cosine = (
        1.0
        - 0.5 * square
        + square
        * square
        * (
            4.166664568298827e-2
            + square * (-1.388731625493765e-3 + square * 2.443315711809948e-5)
        )
    )
    quarter = turns.astype(jnp.int32)
    odd = (quarter & 1) == 1
    out_cos = jnp.where(odd, sine, cosine)
    out_sin = jnp.where(odd, cosine, sine)
    out_cos = jnp.where(((quarter + 1) & 2) == 2, -out_cos, out_cos)
    out_sin = jnp.where((quarter & 2) == 2, -out_sin, out_sin)
    return out_cos, out_sin


def one_minus_exp_neg(y):
    series = y * (
        1.0
        - y * (1.0 / 2)
        * (1.0 - y * (1.0 / 3) * (1.0 - y * (1.0 / 4) * (1.0 - y * (1.0 / 5) * (1.0 - y * (1.0 / 6)))))
    )
    return jnp.where(y < 0.3, series, 1.0 - jnp.exp(-y))


def dot(a, b, dims=((1,), (0,)), precision=None):
    return lax.dot_general(a, b, (dims, ((), ())), preferred_element_type=f32, precision=precision)


def iota(shape, axis):
    return lax.broadcasted_iota(jnp.int32, shape, axis)


def ones_where(condition, dtype=bf16):
    return jnp.where(condition, 1.0, 0.0).astype(dtype)


def scaled_rows(values, gain):
    widened = values.astype(f32)
    factor = lax.rsqrt(jnp.mean(widened * widened, axis=-1, keepdims=True) + eps_norm)
    return (widened * factor * gain).astype(bf16)


def body(
    n_ep, n_tp,
    u_hbm, logs_hbm, loss_hbm, eig_hbm, freq_hbm, gin_hbm, gout_hbm, feed_hbm, mscale_hbm, mweight_hbm,
    x_hbm, gain_hbm, routes_hbm, chosen_hbm, gate_hbm, up_hbm, down_hbm, sgate_hbm, sup_hbm, sdown_hbm,
    mixed_ref, moe_ref,
    u, logs, loss, eig, freq, gin, gout, feed, mscale, mweight,
    x, gain, routes, chosen, gate, up, down, sgate, sup, sdown,
    tok, hid, res, ret, ends, ssm,
    us, parts, eigrow, freqrow, win, wout, ar_ref, ai_ref, br_ref, bi_ref, pre, inc, total, shared_cols, shares,
    load_sem,
    tok_up, tok_dn, tok_x, tok_sib, tok_recv, tok_recv_sib,
    hid_send_y, hid_send_sib, hid_recv_y, hid_recv_sib,
    res_send, res_recv, ends_send, ends_recv,
    ssm_sem,
):
    e, t = lax.axis_index("ep"), lax.axis_index("tp")
    n_line, n_y = n_ep // 2, n_tp // 2
    a, b = e // 2, e % 2
    y, c = t // 2, t % 2
    steps = n_ep
    token_rows, width = x.shape
    half = width // 2
    hidden = gate.shape[1]
    columns = down.shape[1]
    positions, channels = u.shape
    groups, states = eig.shape
    group_ch = channels // groups
    lanes_all = groups * states
    tiles = lanes_all // LANES
    per_tile = LANES // states
    segment = positions // ROWS

    barrier = pltpu.get_barrier_semaphore()
    for i in range(n_ep):
        @pl.when(e != i)
        def _():
            pl.semaphore_signal(barrier, inc=1, device_id={"ep": i, "tp": t}, device_id_type=MESH)
    for i in range(n_tp):
        @pl.when(t != i)
        def _():
            pl.semaphore_signal(barrier, inc=1, device_id={"ep": e, "tp": i}, device_id_type=MESH)

    pairs = [
        (x_hbm, x), (gain_hbm, gain), (sgate_hbm, sgate), (sup_hbm, sup), (gate_hbm.at[0], gate), (up_hbm.at[0], up),
        (u_hbm, u), (logs_hbm, logs), (loss_hbm, loss), (eig_hbm, eig), (freq_hbm, freq), (gin_hbm, gin),
        (gout_hbm, gout), (feed_hbm, feed), (down_hbm.at[0], down), (sdown_hbm, sdown), (mscale_hbm, mscale),
        (mweight_hbm, mweight), (routes_hbm, routes), (chosen_hbm, chosen),
    ]
    loads = [pltpu.make_async_copy(src, dst, load_sem.at[k]) for k, (src, dst) in enumerate(pairs)]
    for load in loads:
        load.start()

    left, right = a, n_line - 1 - a
    short = jnp.minimum(left, right)
    sign_long = jnp.where(left <= right, 1, -1)

    def near(k):
        odd = k % 2
        alternating = jnp.where(odd == 1, sign_long, -sign_long) * ((k + 1) // 2)
        beyond = sign_long * (k - short)
        return a + jnp.where(k <= 2 * short, alternating, beyond)

    def place(s):
        last = s == steps - 1
        odd = s % 2 == 1
        k = jnp.where(last, n_line - 1, jnp.where(odd, (s + 1) // 2, s // 2 - 1))
        other = jnp.where(last, 1, jnp.where(odd, 0, 1))
        k = jnp.where(s == 0, 0, k)
        other = jnp.where(s == 0, 0, other)
        row = jnp.where(k == 0, a, near(k))
        return row, other

    def block_of(row, other):
        return row * 2 + jnp.where(other == 1, 1 - b, b)

    def token_copy(blk, half_index, send, recv, ep, tp):
        part = tok.at[blk, :, pl.ds(pl.multiple_of(half_index * half, half), half)]
        return pltpu.make_async_remote_copy(
            part, part, send, recv, device_id={"ep": ep, "tp": tp}, device_id_type=MESH
        )

    sib = y * 2 + 1 - c

    def up_copy(row):
        return token_copy(row * 2 + b, c, tok_up.at[row], tok_recv.at[row * 2 + b], jnp.minimum(e + 2, n_ep - 2 + b), t)

    def dn_copy(row):
        return token_copy(row * 2 + b, c, tok_dn.at[row], tok_recv.at[row * 2 + b], jnp.maximum(e - 2, b), t)

    def x_copy(row):
        return token_copy(row * 2 + b, c, tok_x.at[row], tok_recv.at[row * 2 + b], a * 2 + 1 - b, t)

    def sib_copy(blk):
        return token_copy(blk, c, tok_sib.at[blk], tok_recv_sib.at[blk], e, sib)

    def forward(row):
        @pl.when((row <= a) & (a + 1 < n_line))
        def _():
            up_copy(row).start()

        @pl.when((row >= a) & (a >= 1))
        def _():
            dn_copy(row).start()

        x_copy(row).start()

    def hid_y_copy(s, yy):
        part = hid.at[s, c, y]
        return pltpu.make_async_remote_copy(
            part, part, hid_send_y.at[s], hid_recv_y.at[s], device_id={"ep": e, "tp": yy * 2 + c}, device_id_type=MESH
        )

    def hid_sib_copy(s, yy):
        part = hid.at[s, c, yy]
        return pltpu.make_async_remote_copy(
            part, part, hid_send_sib.at[s], hid_recv_sib.at[s], device_id={"ep": e, "tp": sib}, device_id_type=MESH
        )

    def span(ref, send, recv):
        return pltpu.make_async_remote_copy(
            ref, ref, send, recv, device_id={"ep": e, "tp": sib}, device_id_type=MESH
        )

    def gated(rows, gate_w, up_w, s):
        block = min(256, hidden)
        for n in range(hidden // block):
            cols = pl.ds(n * block, block)
            gate_part = dot(rows, gate_w[:, cols])
            up_part = dot(rows, up_w[:, cols])
            hid[s, c, y, :, cols] = (gate_part / (1.0 + jnp.exp(-gate_part)) * up_part).astype(bf16)

    def send_hidden(s):
        for dy in range(1, n_y):
            hid_y_copy(s, lax.rem(y + dy, n_y)).start()
        hid_sib_copy(s, y).start()

    def relay_hidden(s):
        span(hid.at[s, c, pl.ds(0, n_y - 1)], hid_send_y.at[s], hid_recv_y.at[s]).wait_recv()
        for dy in range(1, n_y):
            hid_sib_copy(s, lax.rem(y + dy, n_y)).start()

    def down_product(s, weight):
        span(hid.at[s, 1 - c], hid_send_sib.at[s], hid_recv_sib.at[s]).wait_recv()
        value = None
        for cc in range(2):
            for yy in range(n_y):
                rows = (yy * 2 + cc) * hidden
                term = dot(hid[s, cc, yy], weight[rows : rows + hidden, :])
                value = term if value is None else value + term
        return value

    def res_copy(blk):
        return pltpu.make_async_remote_copy(
            res.at[blk], ret.at[e], res_send.at[blk], res_recv.at[e], device_id={"ep": blk, "tp": t}, device_id_type=MESH
        )

    loads[0].wait()
    loads[1].wait()
    tok[e] = scaled_rows(x[...], gain[...])
    pl.semaphore_wait(barrier, n_ep + n_tp - 2)
    forward(a)

    loads[2].wait()
    loads[3].wait()
    gated(tok[e], sgate, sup, steps)
    send_hidden(steps)
    loads[4].wait()
    loads[5].wait()
    gated(tok[e], gate, up, 0)
    send_hidden(0)

    for k in range(6, 14):
        loads[k].wait()
    shuffle = ones_where(iota((positions, positions), 1) == (iota((positions, positions), 0) % ROWS) * segment + iota((positions, positions), 0) // ROWS)
    us[...] = dot(shuffle, u[...]).astype(bf16)
    parts[...] = jnp.zeros(parts.shape, bf16)
    slot = parts.shape[1] // 3
    for q, table in enumerate((jnp.exp(logs[...]), loss[...])):
        rest = table
        for r in range(3):
            piece = rest.astype(bf16)
            rest = rest - piece.astype(f32)
            parts[q, r * slot : r * slot + groups, :] = dot(piece, shuffle, ((1,), (1,))).astype(bf16)
    spread = ones_where(iota((states, LANES), 1) % states == iota((states, LANES), 0), f32)
    for table, rows_ref in ((eig, eigrow), (freq, freqrow)):
        wide = dot(table[...], spread, precision=lax.Precision.HIGHEST)
        row = jnp.zeros((tiles, LANES), f32)
        for h in range(per_tile):
            pick = ones_where(iota((tiles, groups), 1) == iota((tiles, groups), 0) * per_tile + h, f32)
            picked = dot(pick, wide, precision=lax.Precision.HIGHEST)
            row = jnp.where(iota((tiles, LANES), 1) // states == h, picked, row)
        rows_ref[...] = row
    spread_all = ones_where(iota((states, lanes_all), 1) % states == iota((states, lanes_all), 0))
    own_group = iota((channels, lanes_all), 0) // group_ch == iota((channels, lanes_all), 1) // states
    for r in range(2):
        win[r] = jnp.where(own_group, dot(gin[r], spread_all), 0.0).astype(bf16)
        wout[r] = jnp.where(own_group, dot(gout[r], spread_all), 0.0).astype(bf16)

    def tile_work(i):
        lanes = pl.ds(pl.multiple_of(i * LANES, LANES), LANES)
        slot_rows = 3 * slot
        own = iota((slot_rows, LANES), 0) % slot == per_tile * i + iota((slot_rows, LANES), 1) // states
        select = ones_where(own)
        step_wide = dot(parts[0], select, ((0,), (0,)))
        loss_wide = dot(parts[1], select, ((0,), (0,)))
        loss_rate = eigrow[pl.ds(i, 1), :] * step_wide
        magnitude = jnp.exp(loss_wide - loss_rate)
        cosine, sine = cos_sin(freqrow[pl.ds(i, 1), :] * step_wide)
        scaling = jnp.sqrt(one_minus_exp_neg(2.0 * loss_rate))
        ar_ref[:, lanes] = magnitude * cosine
        ai_ref[:, lanes] = magnitude * sine
        br_ref[:, lanes] = scaling * dot(us[...], win[0, :, lanes])
        bi_ref[:, lanes] = scaling * dot(us[...], win[1, :, lanes])
        reach = jnp.ones((ROWS, LANES), f32), jnp.zeros((ROWS, LANES), f32)
        state = jnp.zeros((ROWS, LANES), f32), jnp.zeros((ROWS, LANES), f32)
        for j in range(segment):
            at = pl.ds(j * ROWS, ROWS)
            ar, ai, br, bi = ar_ref[at, lanes], ai_ref[at, lanes], br_ref[at, lanes], bi_ref[at, lanes]
            reach = ar * reach[0] - ai * reach[1], ar * reach[1] + ai * reach[0]
            state = ar * state[0] - ai * state[1] + br, ar * state[1] + ai * state[0] + bi
            ar_ref[at, lanes] = reach[0]
            ai_ref[at, lanes] = reach[1]
            br_ref[at, lanes] = state[0]
            bi_ref[at, lanes] = state[1]
        row = iota((ROWS, LANES), 0)
        er, ei = jnp.ones((1, LANES), f32), jnp.zeros((1, LANES), f32)
        sr, si = jnp.zeros((1, LANES), f32), jnp.zeros((1, LANES), f32)
        pre_r = pre_i = pre_sr = pre_si = jnp.zeros((ROWS, LANES), f32)
        for k in range(ROWS):
            here = row == k
            pre_r = jnp.where(here, er, pre_r)
            pre_i = jnp.where(here, ei, pre_i)
            pre_sr = jnp.where(here, sr, pre_sr)
            pre_si = jnp.where(here, si, pre_si)
            tr, ti = reach[0][k : k + 1], reach[1][k : k + 1]
            ur, ui = state[0][k : k + 1], state[1][k : k + 1]
            er, ei, sr, si = (
                tr * er - ti * ei,
                tr * ei + ti * er,
                tr * sr - ti * si + ur,
                tr * si + ti * sr + ui,
            )
        for q, value in enumerate((pre_r, pre_i, pre_sr, pre_si)):
            pre[q, i] = value
        for q, value in enumerate((er, ei, sr, si)):
            ends[e, q, pl.ds(i, 1), :] = value

    def ends_copy(i):
        return pltpu.make_async_remote_copy(
            ends.at[e], ends.at[e], ends_send.at[i], ends_recv.at[e], device_id={"ep": i, "tp": t}, device_id_type=MESH
        )

    def send_ends():
        for i in range(1, n_ep):
            @pl.when(i > e)
            def _():
                ends_copy(i).start()

    def incoming():
        zero = jnp.zeros((tiles, LANES), f32)
        inc[0] = zero
        inc[1] = zero
        for i in range(n_ep - 1):
            @pl.when(i < e)
            def _():
                part = ends.at[i]
                pltpu.make_async_remote_copy(
                    part, part, ends_send.at[i], ends_recv.at[i], device_id={"ep": e, "tp": sib}, device_id_type=MESH
                ).wait_recv()
                tr, ti, ur, ui = ends[i, 0], ends[i, 1], ends[i, 2], ends[i, 3]
                sr, si = inc[0], inc[1]
                inc[0] = tr * sr - ti * si + ur
                inc[1] = tr * si + ti * sr + ui

    def split(value):
        high = value.astype(bf16)
        return high, (value - high.astype(f32)).astype(bf16)

    def read_tile(i):
        lanes = pl.ds(pl.multiple_of(i * LANES, LANES), LANES)
        ir, ii = inc[0, pl.ds(i, 1), :], inc[1, pl.ds(i, 1), :]
        pre_r, pre_i, pre_sr, pre_si = pre[0, i], pre[1, i], pre[2, i], pre[3, i]
        enter_r = (pre_sr + pre_r * ir - pre_i * ii)[None]
        enter_i = (pre_si + pre_r * ii + pre_i * ir)[None]
        shape = (segment, ROWS, LANES)
        ar, ai = ar_ref[:, lanes].reshape(shape), ai_ref[:, lanes].reshape(shape)
        br, bi = br_ref[:, lanes].reshape(shape), bi_ref[:, lanes].reshape(shape)
        state_r = (br + ar * enter_r - ai * enter_i).reshape(positions, LANES)
        state_i = (bi + ar * enter_i + ai * enter_r).reshape(positions, LANES)
        wr, wi = wout[0, :, lanes], -wout[1, :, lanes]
        high_r, low_r = split(state_r)
        high_i, low_i = split(state_i)
        nt = ((1,), (1,))
        total[...] += (dot(high_r, wr, nt) + dot(low_r, wr, nt)) + (dot(high_i, wi, nt) + dot(low_i, wi, nt))

    def ssm_y_copy(yy):
        part = ssm.at[c, y]
        return pltpu.make_async_remote_copy(
            part, part, ssm_sem.at[0], ssm_sem.at[1], device_id={"ep": e, "tp": yy * 2 + c}, device_id_type=MESH
        )

    def ssm_sib_copy(yy):
        part = ssm.at[c, yy]
        return pltpu.make_async_remote_copy(
            part, part, ssm_sem.at[2], ssm_sem.at[3], device_id={"ep": e, "tp": sib}, device_id_type=MESH
        )

    def read_out():
        total[...] = feed[...] * us[...].astype(f32)
        lax.fori_loop(0, tiles, lambda i, _: (read_tile(i), 0)[1], 0)
        value = total[...]
        inner = 0.7978845608028654 * (value + 0.044715 * (value * value * value))
        result = (0.5 * value * (1.0 + jnp.tanh(inner))).astype(bf16)
        unshuffle = ones_where(iota((positions, positions), 1) == (iota((positions, positions), 0) % segment) * ROWS + iota((positions, positions), 0) // segment)
        ssm[c, y] = dot(unshuffle, result).astype(bf16)
        for dy in range(1, n_y):
            ssm_y_copy(lax.rem(y + dy, n_y)).start()
        ssm_sib_copy(y).start()

    for k in range(14, 20):
        loads[k].wait()

    mixer_steps = -(-tiles // TILES_PER_STEP)
    ends_step = mixer_steps + 1
    read_step = min(ends_step + 2, steps + DOWN_LAG - 1)

    def step_body(s, carry):
        @pl.when(s < steps)
        def _():
            row, other = place(s)
            blk = block_of(row, other)
            token_copy(blk, c, tok_sib.at[blk], tok_recv.at[blk], e, sib).wait_recv()

            @pl.when(other == 0)
            def _():
                forward(row)

            sib_copy(blk).start()

        for k in range(TILES_PER_STEP):
            i = (s - 1) * TILES_PER_STEP + k

            @pl.when(i < tiles)
            def _():
                tile_work(i)

        @pl.when(s == ends_step)
        def _():
            send_ends()

        @pl.when(s < steps)
        def _():
            row, other = place(s)
            blk = block_of(row, other)
            token_copy(blk, 1 - c, tok_sib.at[blk], tok_recv_sib.at[blk], e, sib).wait_recv()
            gated(tok[blk], gate, up, s)
            send_hidden(s)

        @pl.when(s == 1)
        def _():
            relay_hidden(steps)

        @pl.when(s - COLUMN_LAG < steps)
        def _():
            relay_hidden(s - COLUMN_LAG)

        @pl.when(s == read_step)
        def _():
            incoming()
            read_out()

        @pl.when(s >= DOWN_LAG)
        def _():
            row, other = place(s - DOWN_LAG)
            blk = block_of(row, other)
            value = down_product(s - DOWN_LAG, down).astype(bf16)

            @pl.when(blk == e)
            def _():
                ret[e] = value

            @pl.when(blk != e)
            def _():
                res[blk] = value
                res_copy(blk).start()

        return carry

    lax.fori_loop(1, steps + DOWN_LAG, step_body, 0)

    span(ssm.at[c, pl.ds(0, n_y - 1)], ssm_sem.at[0], ssm_sem.at[1]).wait_recv()
    for dy in range(1, n_y):
        ssm_sib_copy(lax.rem(y + dy, n_y)).start()
    shared_cols[...] = down_product(steps, sdown)
    span(ssm.at[1 - c], ssm_sem.at[2], ssm_sem.at[3]).wait_recv()
    squares = jnp.zeros((positions, 1), f32)
    for cc in range(2):
        for yy in range(n_y):
            piece = ssm[cc, yy].astype(f32)
            squares = squares + jnp.sum(piece * piece, axis=-1, keepdims=True)
    factor = lax.rsqrt(squares / (channels * n_tp) + eps_norm)

    def gain_of(tt):
        if channels % LANES == 0:
            return mscale[:, tt * channels : (tt + 1) * channels]
        return mscale[tt : tt + 1, :]

    value = None
    for cc in range(2):
        for yy in range(n_y):
            tt = yy * 2 + cc
            normed = (ssm[cc, yy].astype(f32) * factor * gain_of(tt)).astype(bf16)
            term = dot(normed, mweight[tt * channels : (tt + 1) * channels, :])
            value = term if value is None else value + term
    mixed_ref[...] = value.astype(bf16)

    taken = jnp.zeros((n_ep, token_rows), f32)
    for k in range(routes.shape[0]):
        taken = taken + jnp.where(iota((n_ep, token_rows), 0) == routes[k : k + 1, :], chosen[k : k + 1, :], 0.0)
    shares[...] = taken.T

    def combine(s, carry):
        row, other = place(s)
        i = block_of(row, other)

        @pl.when(i != e)
        def _():
            part = ret.at[i]
            pltpu.make_async_remote_copy(
                part, part, res_send.at[i], res_recv.at[i], device_id={"ep": e, "tp": sib}, device_id_type=MESH
            ).wait_recv()

        share = jnp.sum(jnp.where(iota((token_rows, n_ep), 1) == i, shares[...], 0.0), axis=1, keepdims=True)
        shared_cols[...] += ret[i].astype(f32) * share
        return carry

    lax.fori_loop(0, steps, combine, 0)
    moe_ref[...] = shared_cols[...].astype(bf16)

    def drain(s, carry):
        @pl.when(s != e)
        def _():
            token_copy(s, c, tok_sib.at[s], tok_recv_sib.at[s], e, sib).wait_send()
            res_copy(s).wait_send()

        @pl.when(s > e)
        def _():
            ends_copy(s).wait_send()

        return carry

    lax.fori_loop(0, n_ep, drain, 0)

    def drain_line(row, carry):
        @pl.when((row <= a) & (a + 1 < n_line))
        def _():
            up_copy(row).wait_send()

        @pl.when((row >= a) & (a >= 1))
        def _():
            dn_copy(row).wait_send()

        x_copy(row).wait_send()
        return carry

    lax.fori_loop(0, n_line, drain_line, 0)

    def drain_hidden(s, carry):
        span(hid.at[s, c, pl.ds(0, n_y - 1)], hid_send_y.at[s], hid_recv_y.at[s]).wait_send()
        span(hid.at[s, c], hid_send_sib.at[s], hid_recv_sib.at[s]).wait_send()
        return carry

    lax.fori_loop(0, steps + 1, drain_hidden, 0)
    span(ssm.at[c, pl.ds(0, n_y - 1)], ssm_sem.at[0], ssm_sem.at[1]).wait_send()
    span(ssm.at[c], ssm_sem.at[2], ssm_sem.at[3]).wait_send()


def on_device(*operands):
    (
        u, logs, losses, eigen, frequency, group_in, group_out, feed, mixer_scale, mixer_weight,
        x, gain, routes, chosen, gate, up, down, shared_gate, shared_up, shared_down,
    ) = operands
    n_ep, n_tp = lax.axis_size("ep"), lax.axis_size("tp")
    positions, channels = u.shape
    groups, states = eigen.shape
    lanes_all = groups * states
    tiles = lanes_all // LANES
    token_rows, width = x.shape
    hidden, columns = gate.shape[2], down.shape[2]
    group_in = group_in.transpose(0, 1, 3, 2).reshape(2, channels, states)
    group_out = group_out.reshape(2, channels, states)
    feed = feed.reshape(1, channels)
    mixer_scale = mixer_scale.reshape((1, -1) if channels % LANES == 0 else (n_tp, channels))
    gain = gain.reshape(1, width)
    routes, chosen = routes.T, chosen.T
    given = (
        u, logs, losses, eigen, frequency, group_in, group_out, feed, mixer_scale, mixer_weight,
        x, gain, routes, chosen, gate, up, down, shared_gate, shared_up, shared_down,
    )
    local = [
        pltpu.VMEM(g.shape[1:] if k in (14, 15, 16) else g.shape, g.dtype) for k, g in enumerate(given)
    ]
    slot = -(-groups // 16) * 16
    wide = pltpu.VMEM((positions, lanes_all), f32)
    dma = pltpu.SemaphoreType.DMA
    scratch = local + [
        pltpu.VMEM((n_ep, token_rows, width), bf16),
        pltpu.VMEM((n_ep + 1, 2, n_tp // 2, token_rows, hidden), bf16),
        pltpu.VMEM((n_ep, token_rows, columns), bf16),
        pltpu.VMEM((n_ep, token_rows, columns), bf16),
        pltpu.VMEM((n_ep, 4, tiles, LANES), f32),
        pltpu.VMEM((2, n_tp // 2, positions, channels), bf16),
        pltpu.VMEM((positions, channels), bf16),
        pltpu.VMEM((2, 3 * slot, positions), bf16),
        pltpu.VMEM((tiles, LANES), f32),
        pltpu.VMEM((tiles, LANES), f32),
        pltpu.VMEM((2, channels, lanes_all), bf16),
        pltpu.VMEM((2, channels, lanes_all), bf16),
        wide, wide, wide, wide,
        pltpu.VMEM((4, tiles, ROWS, LANES), f32),
        pltpu.VMEM((2, tiles, LANES), f32),
        pltpu.VMEM((positions, channels), f32),
        pltpu.VMEM((token_rows, columns), f32),
        pltpu.VMEM((token_rows, n_ep), f32),
        dma((len(given),)),
        dma((n_ep // 2,)), dma((n_ep // 2,)), dma((n_ep // 2,)), dma((n_ep,)), dma((n_ep,)), dma((n_ep,)),
        dma((n_ep + 1,)), dma((n_ep + 1,)), dma((n_ep + 1,)), dma((n_ep + 1,)),
        dma((n_ep,)), dma((n_ep,)), dma((n_ep,)), dma((n_ep,)),
        dma((4,)),
    ]
    return pl.pallas_call(
        functools.partial(body, n_ep, n_tp),
        out_shape=[
            jax.ShapeDtypeStruct((positions, columns), bf16),
            jax.ShapeDtypeStruct((token_rows, columns), bf16),
        ],
        in_specs=[pl.BlockSpec(memory_space=pl.ANY)] * len(given),
        out_specs=[pl.BlockSpec(memory_space=pltpu.VMEM)] * 2,
        scratch_shapes=scratch,
        compiler_params=pltpu.CompilerParams(
            collective_id=0, has_side_effects=True, vmem_limit_bytes=VMEM_BYTES
        ),
        name="both_batches",
    )(*given)


def solution(mesh):
    return jax.shard_map(
        on_device,
        mesh=mesh,
        in_specs=(
            P("ep", "tp"),
            P("tp", "ep"),
            P("tp", "ep"),
            P("tp", None),
            P("tp", None),
            P(None, "tp", None, None),
            P(None, "tp", None, None),
            P("tp"),
            P(),
            P(None, "tp"),
            P("ep", None),
            P(),
            P("ep", None),
            P("ep", None),
            P("ep", None, "tp"),
            P("ep", None, "tp"),
            P("ep", None, "tp"),
            P(None, "tp"),
            P(None, "tp"),
            P(None, "tp"),
        ),
        out_specs=(P("ep", "tp"), P("ep", "tp")),
        check_vma=False,
    )
```

time: 228 us -> 69.2 us (0.30)
  waiting for transfers between devices: 65.7 us -> 0 us
  blocking collectives: 63.4 us -> 0 us
  Pallas kernels: 16.6 us -> 65.1 us
  local copies, waits for them, and re-layouts: 34.7 us -> 3.24 us
  matrix products: 21.2 us -> 0 us
  between operations: 14 us -> 0.65 us
  starting transfers between devices: 6.07 us -> 0 us
  other arithmetic: 5.42 us -> 0 us
    all_gather x3 -> x0, waiting for transfers between devices: 65.6 us -> none  [the longest x1 51.9 us: on_device(): half_tokens = lax.all_gather(own_half, 'ep', axis=0, tiled=True)]
    all_gather x3 -> x0, blocking collectives: 63.4 us -> none  [the longest x1 48.4 us: mixer_local(): all_ends = lax.all_gather(ends, 'ep')]
    pallas_call x2 -> x1, Pallas kernels: 16.6 us -> 65.1 us  [on_device(): pl.pallas_call(functools.partial(body, n_ep, n_tp), out_shape=[jax.ShapeD...]
    dot_general x7 -> x0, matrix products: 21.2 us -> none  [the longest x1 6.17 us: on_device(): jnp.dot(whole_hidden, down_weight, preferred_element_type=jnp.float32)]
    broadcast_in_dim x10 -> x0, local copies, waits for them, and re-layouts: 20.3 us -> none  [the longest x6 14.4 us: mixer_local(): jnp.where(same[None, :, None, :, None], group_out.transpose(0, 1, 3, 2)[:...]
    reshape x8 -> x0, local copies, waits for them, and re-layouts: 6.22 us -> none  [the longest x5 2.57 us: shuffled(): return rows.reshape(ROWS, seg, -1).transpose(1, 0, 2).reshape(positions, -1)]
    all_to_all x1 -> x0, starting transfers between devices: 5.96 us -> none  [on_device(): lax.all_to_all(results, 'ep', split_axis=0, concat_axis=0, tiled=True)]
    another operation x4 -> x0, local copies, waits for them, and re-layouts: 5.09 us -> none  [by_tile(): wide = shuffled(table.T).reshape(positions, tiles, per_tile)]
  transfers between devices with their start and end apart: 4 -> 0, of which waited for: 2 -> 0; matrix products, arithmetic and copies ran while one was open for 17% -> 0% of each run, Pallas kernels for 7% -> 0%
where the time goes in v1:
time: 69.2 us; the launch traced here: 69 us
  Pallas kernels  65.1 us (94%)
  local copies, waits for them, and re-layouts  3.24 us (5%)
    pallas_call x1, Pallas kernels, on_device(): pl.pallas_call(functools.partial(body, n_ep, n_tp), out_shape=[jax.ShapeD...  65.1 us
    unnamed x2, local copies, waits for them, and re-layouts  3.24 us

profile of v1, /device:TPU:0, one launch (start us, length us, event | category | flops | bytes accessed | tf_op | source)
XLA Modules:
  0.0 69.0 jit_solution(10924387945268954399)
XLA Ops:
  0.6 65.1 %both_batches.1 = (bf16[256,512]{1,0:T(8,128)(2,1)}, bf16[128,512]{1,0:T(8,128)(2,1)}) custom-call(bf16[256,256]{1,0:T(8,128)(2,1)} %u_hbm.1, f32[16,256]{1,0:T(8,128)} %logs_hbm.1, f32[16,256]{1,0:T(8,128)} %loss_hbm.1, f32[16,64]{1,0:T(8,128)} %eig_hbm.1, f32[16,64]{1,0:T(8,128)} %freq_hbm.1, bf16[2,256,64]{2,1,0:T(8,128)(2,1)} %bitcast.9, ...), custom_call_target="tpu_custom_call" | custom-call | tf_op jit(solution)/shard_map/both_batches/pallas_call | solution.py:604
  65.8 1.7 %copy.24 = bf16[256,512]{1,0:T(8,128)(2,1)} copy(bf16[256,512]{1,0:T(8,128)(2,1)} %get-tuple-element.4) | data formatting | bytes 524288
  67.4 1.6 %copy.25 = bf16[128,512]{1,0:T(8,128)(2,1)} copy(bf16[128,512]{1,0:T(8,128)(2,1)} %get-tuple-element.5) | data formatting | bytes 262144

commit v2 on v1

--- a/solution.py
+++ b/solution.py
@@ -12,9 +12,7 @@
 ROWS = 8
 MESH = pl.DeviceIdType.MESH
 bf16, f32 = jnp.bfloat16, jnp.float32
-COLUMN_LAG = 1
-DOWN_LAG = 2
-TILES_PER_STEP = 2
+EARLY_TILES = 4
 VMEM_BYTES = 62 * 1024 * 1024
 
 
@@ -75,7 +73,7 @@
     n_ep, n_tp,
     u_hbm, logs_hbm, loss_hbm, eig_hbm, freq_hbm, gin_hbm, gout_hbm, feed_hbm, mscale_hbm, mweight_hbm,
     x_hbm, gain_hbm, routes_hbm, chosen_hbm, gate_hbm, up_hbm, down_hbm, sgate_hbm, sup_hbm, sdown_hbm,
-    mixed_ref, moe_ref,
+    mixed_hbm, moe_hbm,
     u, logs, loss, eig, freq, gin, gout, feed, mscale, mweight,
     x, gain, routes, chosen, gate, up, down, sgate, sup, sdown,
     tok, hid, res, ret, ends, ssm,
@@ -84,7 +82,7 @@
     tok_up, tok_dn, tok_x, tok_sib, tok_recv, tok_recv_sib,
     hid_send_y, hid_send_sib, hid_recv_y, hid_recv_sib,
     res_send, res_recv, ends_send, ends_recv,
-    ssm_sem,
+    ssm_sem, store_sem, mixed_ref, moe_ref,
 ):
     e, t = lax.axis_index("ep"), lax.axis_index("tp")
     n_line, n_y = n_ep // 2, n_tp // 2
@@ -138,6 +136,10 @@
         odd = s % 2 == 1
         k = jnp.where(last, n_line - 1, jnp.where(odd, (s + 1) // 2, s // 2 - 1))
         other = jnp.where(last, 1, jnp.where(odd, 0, 1))
+        own_first = short >= 1
+        swapped = jnp.where(s == n_line, 1, jnp.where(s == n_line + 1, 0, s - n_line))
+        k = jnp.where(own_first, jnp.where(s < n_line, s, swapped), k)
+        other = jnp.where(own_first, jnp.where(s < n_line, 0, 1), other)
         k = jnp.where(s == 0, 0, k)
         other = jnp.where(s == 0, 0, other)
         row = jnp.where(k == 0, a, near(k))
@@ -393,78 +395,112 @@
     for k in range(14, 20):
         loads[k].wait()
 
-    mixer_steps = -(-tiles // TILES_PER_STEP)
-    ends_step = mixer_steps + 1
-    read_step = min(ends_step + 2, steps + DOWN_LAG - 1)
-
-    def step_body(s, carry):
-        @pl.when(s < steps)
-        def _():
-            row, other = place(s)
-            blk = block_of(row, other)
-            token_copy(blk, c, tok_sib.at[blk], tok_recv.at[blk], e, sib).wait_recv()
-
-            @pl.when(other == 0)
-            def _():
-                forward(row)
-
-            sib_copy(blk).start()
-
-        for k in range(TILES_PER_STEP):
-            i = (s - 1) * TILES_PER_STEP + k
-
-            @pl.when(i < tiles)
-            def _():
-                tile_work(i)
-
-        @pl.when(s == ends_step)
+    early = min(EARLY_TILES, tiles)
+    lax.fori_loop(0, early, lambda i, _: (tile_work(i), 0)[1], 0)
+
+    def arrive(s):
+        row, other = place(s)
+        blk = block_of(row, other)
+        token_copy(blk, c, tok_sib.at[blk], tok_recv.at[blk], e, sib).wait_recv()
+
+        @pl.when(other == 0)
+        def _():
+            forward(row)
+
+        sib_copy(blk).start()
+
+    def first_products(s):
+        row, other = place(s)
+        blk = block_of(row, other)
+        token_copy(blk, 1 - c, tok_sib.at[blk], tok_recv_sib.at[blk], e, sib).wait_recv()
+        gated(tok[blk], gate, up, s)
+        send_hidden(s)
+
+    def held(s):
+        return (s == 2) & (short < 1) & (steps >= 6)
+
+    def last_product(s):
+        row, other = place(s)
+        blk = block_of(row, other)
+        value = down_product(s, down).astype(bf16)
+
+        @pl.when(blk == e)
+        def _():
+            ret[e] = value
+
+        @pl.when(blk != e)
+        def _():
+            res[blk] = value
+
+        @pl.when((blk != e) & jnp.logical_not(held(s)))
+        def _():
+            res_copy(blk).start()
+
+    last_pair = steps // 2
+
+    def one(q, act):
+        @pl.when((q >= 0) & (q < steps))
+        def _():
+            act(q)
+
+    def pair(p, carry):
+        one(2 * p - 1, arrive)
+        one(2 * p, arrive)
+
+        @pl.when((p == 3) & (short < 1) & (steps >= 6))
+        def _():
+            row, other = place(2)
+            res_copy(block_of(row, other)).start()
+
+        one(2 * p - 1, first_products)
+
+        @pl.when(p != last_pair)
+        def _():
+            one(2 * p - 3, relay_hidden)
+
+        @pl.when(p == last_pair)
+        def _():
+            one(2 * p - 3, last_product)
+
+        one(2 * p, first_products)
+        one(2 * p - 2, relay_hidden)
+
+        @pl.when(p == 1)
+        def _():
+            relay_hidden(steps)
+
+        @pl.when(p <= 2)
+        def _():
+            middle = (early + tiles) // 2
+            lax.fori_loop(jnp.where(p == 1, early, middle), jnp.where(p == 1, middle, tiles), lambda i, _: (tile_work(i), 0)[1], 0)
+
+        @pl.when(p == 2)
         def _():
             send_ends()
 
-        @pl.when(s < steps)
-        def _():
-            row, other = place(s)
-            blk = block_of(row, other)
-            token_copy(blk, 1 - c, tok_sib.at[blk], tok_recv_sib.at[blk], e, sib).wait_recv()
-            gated(tok[blk], gate, up, s)
-            send_hidden(s)
-
-        @pl.when(s == 1)
-        def _():
-            relay_hidden(steps)
-
-        @pl.when(s - COLUMN_LAG < steps)
-        def _():
-            relay_hidden(s - COLUMN_LAG)
-
-        @pl.when(s == read_step)
+        @pl.when(p != last_pair)
+        def _():
+            one(2 * p - 3, last_product)
+
+        one(2 * p - 2, last_product)
+
+        @pl.when(p == last_pair - 1)
         def _():
             incoming()
             read_out()
-
-        @pl.when(s >= DOWN_LAG)
-        def _():
-            row, other = place(s - DOWN_LAG)
-            blk = block_of(row, other)
-            value = down_product(s - DOWN_LAG, down).astype(bf16)
-
-            @pl.when(blk == e)
-            def _():
-                ret[e] = value
-
-            @pl.when(blk != e)
-            def _():
-                res[blk] = value
-                res_copy(blk).start()
+            one(2 * p - 1, relay_hidden)
+
+        @pl.when(p == last_pair)
+        def _():
+            span(ssm.at[c, pl.ds(0, n_y - 1)], ssm_sem.at[0], ssm_sem.at[1]).wait_recv()
+            for dy in range(1, n_y):
+                ssm_sib_copy(lax.rem(y + dy, n_y)).start()
+            shared_cols[...] = down_product(steps, sdown)
 
         return carry
 
-    lax.fori_loop(1, steps + DOWN_LAG, step_body, 0)
-
-    span(ssm.at[c, pl.ds(0, n_y - 1)], ssm_sem.at[0], ssm_sem.at[1]).wait_recv()
-    for dy in range(1, n_y):
-        ssm_sib_copy(lax.rem(y + dy, n_y)).start()
-    shared_cols[...] = down_product(steps, sdown)
+    lax.fori_loop(1, steps // 2 + 2, pair, 0)
+
     span(ssm.at[1 - c], ssm_sem.at[2], ssm_sem.at[3]).wait_recv()
     squares = jnp.zeros((positions, 1), f32)
     for cc in range(2):
@@ -486,6 +522,8 @@
             term = dot(normed, mweight[tt * channels : (tt + 1) * channels, :])
             value = term if value is None else value + term
     mixed_ref[...] = value.astype(bf16)
+    mixed_store = pltpu.make_async_copy(mixed_ref, mixed_hbm, store_sem.at[0])
+    mixed_store.start()
 
     taken = jnp.zeros((n_ep, token_rows), f32)
     for k in range(routes.shape[0]):
@@ -509,6 +547,8 @@
 
     lax.fori_loop(0, steps, combine, 0)
     moe_ref[...] = shared_cols[...].astype(bf16)
+    moe_store = pltpu.make_async_copy(moe_ref, moe_hbm, store_sem.at[1])
+    moe_store.start()
 
     def drain(s, carry):
         @pl.when(s != e)
@@ -546,6 +586,24 @@
     lax.fori_loop(0, steps + 1, drain_hidden, 0)
     span(ssm.at[c, pl.ds(0, n_y - 1)], ssm_sem.at[0], ssm_sem.at[1]).wait_send()
     span(ssm.at[c], ssm_sem.at[2], ssm_sem.at[3]).wait_send()
+    mixed_store.wait()
+    moe_store.wait()
+
+
+def hand_over(mixed, moe_out):
+    def copy(mixed_in, moe_in, mixed_ref, moe_ref):
+        mixed_ref[...] = mixed_in[...]
+        moe_ref[...] = moe_in[...]
+
+    specs = [pl.BlockSpec(v.shape, lambda i: (0, 0)) for v in (mixed, moe_out)]
+    return pl.pallas_call(
+        copy,
+        grid=(1,),
+        in_specs=specs,
+        out_specs=specs,
+        out_shape=[jax.ShapeDtypeStruct(v.shape, v.dtype) for v in (mixed, moe_out)],
+        name="hand_over",
+    )(mixed, moe_out)
 
 
 def on_device(*operands):
@@ -600,21 +658,25 @@
         dma((n_ep + 1,)), dma((n_ep + 1,)), dma((n_ep + 1,)), dma((n_ep + 1,)),
         dma((n_ep,)), dma((n_ep,)), dma((n_ep,)), dma((n_ep,)),
         dma((4,)),
+        dma((2,)),
+        pltpu.VMEM((positions, columns), bf16),
+        pltpu.VMEM((token_rows, columns), bf16),
     ]
-    return pl.pallas_call(
+    mixed, moe_out = pl.pallas_call(
         functools.partial(body, n_ep, n_tp),
         out_shape=[
             jax.ShapeDtypeStruct((positions, columns), bf16),
             jax.ShapeDtypeStruct((token_rows, columns), bf16),
         ],
         in_specs=[pl.BlockSpec(memory_space=pl.ANY)] * len(given),
-        out_specs=[pl.BlockSpec(memory_space=pltpu.VMEM)] * 2,
+        out_specs=[pl.BlockSpec(memory_space=pl.ANY)] * 2,
         scratch_shapes=scratch,
         compiler_params=pltpu.CompilerParams(
             collective_id=0, has_side_effects=True, vmem_limit_bytes=VMEM_BYTES
         ),
         name="both_batches",
     )(*given)
+    return hand_over(mixed, moe_out)
 
 
 def solution(mesh):

time: 69.2 us -> 56.7 us (0.82)
  Pallas kernels: 65.1 us -> 55.9 us
  local copies, waits for them, and re-layouts: 3.24 us -> 0 us
    pallas_call x1, Pallas kernels: 65.1 us -> 54.2 us  [on_device(): pl.pallas_call(functools.partial(body, n_ep, n_tp), out_shape=[jax.ShapeD...]
    unnamed x2 -> x0, local copies, waits for them, and re-layouts: 3.24 us -> none
    pallas_call x0 -> x1, Pallas kernels: none -> 1.74 us  [hand_over(): pl.pallas_call(copy, grid=(1,), in_specs=specs, out_specs=specs, out_shap...]
where the time goes in v2:
time: 56.7 us; the launch traced here: 56.6 us
  Pallas kernels  55.9 us (99%)
  between operations  0.65 us (1%)
    pallas_call x1, Pallas kernels, on_device(): pl.pallas_call(functools.partial(body, n_ep, n_tp), out_shape=[jax.ShapeD...  54.2 us
    pallas_call x1, Pallas kernels, hand_over(): pl.pallas_call(copy, grid=(1,), in_specs=specs, out_specs=specs, out_shap...  1.74 us

profile of v2, /device:TPU:0, one launch (start us, length us, event | category | flops | bytes accessed | tf_op | source)
XLA Modules:
  0.0 56.6 jit_solution(261056284460064622)
XLA Ops:
  0.6 54.2 %both_batches.1 = (bf16[256,512]{1,0:T(8,128)(2,1)}, bf16[128,512]{1,0:T(8,128)(2,1)}) custom-call(bf16[256,256]{1,0:T(8,128)(2,1)} %u_hbm.1, f32[16,256]{1,0:T(8,128)} %logs_hbm.1, f32[16,256]{1,0:T(8,128)} %loss_hbm.1, f32[16,64]{1,0:T(8,128)} %eig_hbm.1, f32[16,64]{1,0:T(8,128)} %freq_hbm.1, bf16[2,256,64]{2,1,0:T(8,128)(2,1)} %bitcast.9, ...), custom_call_target="tpu_custom_call" | custom-call | tf_op jit(solution)/shard_map/both_batches/pallas_call | solution.py:665
  54.8 1.7 %hand_over.1 = (bf16[256,512]{1,0:T(8,128)(2,1)}, bf16[128,512]{1,0:T(8,128)(2,1)}) custom-call(bf16[256,512]{1,0:T(8,128)(2,1)} %get-tuple-element.4.mixed_in, bf16[128,512]{1,0:T(8,128)(2,1)} %get-tuple-element.5.moe_in), custom_call_target="tpu_custom_call" | custom-call | tf_op jit(solution)/shard_map/hand_over/pallas_call | solution.py:599

commit v3 on v2

--- a/solution.py
+++ b/solution.py
@@ -12,7 +12,8 @@
 ROWS = 8
 MESH = pl.DeviceIdType.MESH
 bf16, f32 = jnp.bfloat16, jnp.float32
-EARLY_TILES = 4
+PIECES = 2
+TILES_IN_FIRST = 6
 VMEM_BYTES = 62 * 1024 * 1024
 
 
@@ -73,16 +74,16 @@
     n_ep, n_tp,
     u_hbm, logs_hbm, loss_hbm, eig_hbm, freq_hbm, gin_hbm, gout_hbm, feed_hbm, mscale_hbm, mweight_hbm,
     x_hbm, gain_hbm, routes_hbm, chosen_hbm, gate_hbm, up_hbm, down_hbm, sgate_hbm, sup_hbm, sdown_hbm,
-    mixed_hbm, moe_hbm,
+    mixed_hbm, sum_hbm, late_hbm, weight_hbm,
     u, logs, loss, eig, freq, gin, gout, feed, mscale, mweight,
     x, gain, routes, chosen, gate, up, down, sgate, sup, sdown,
     tok, hid, res, ret, ends, ssm,
-    us, parts, eigrow, freqrow, win, wout, ar_ref, ai_ref, br_ref, bi_ref, pre, inc, total, shared_cols, shares,
+    us, parts, eigrow, freqrow, win, wout, ar_ref, ai_ref, br_ref, bi_ref, whole, pre, inc, total, shared_cols, shares,
     load_sem,
     tok_up, tok_dn, tok_x, tok_sib, tok_recv, tok_recv_sib,
     hid_send_y, hid_send_sib, hid_recv_y, hid_recv_sib,
     res_send, res_recv, ends_send, ends_recv,
-    ssm_sem, store_sem, mixed_ref, moe_ref,
+    ssm_sem, store_sem, mixed_ref, late_weight,
 ):
     e, t = lax.axis_index("ep"), lax.axis_index("tp")
     n_line, n_y = n_ep // 2, n_tp // 2
@@ -148,47 +149,59 @@
     def block_of(row, other):
         return row * 2 + jnp.where(other == 1, 1 - b, b)
 
-    def token_copy(blk, half_index, send, recv, ep, tp):
-        part = tok.at[blk, :, pl.ds(pl.multiple_of(half_index * half, half), half)]
+    piece_rows = token_rows // PIECES
+
+    def token_copy(blk, piece, half_index, send, recv, ep, tp):
+        rows = pl.ds(pl.multiple_of(piece * piece_rows, piece_rows), piece_rows)
+        part = tok.at[blk, rows, pl.ds(pl.multiple_of(half_index * half, half), half)]
         return pltpu.make_async_remote_copy(
             part, part, send, recv, device_id={"ep": ep, "tp": tp}, device_id_type=MESH
         )
 
     sib = y * 2 + 1 - c
 
-    def up_copy(row):
-        return token_copy(row * 2 + b, c, tok_up.at[row], tok_recv.at[row * 2 + b], jnp.minimum(e + 2, n_ep - 2 + b), t)
-
-    def dn_copy(row):
-        return token_copy(row * 2 + b, c, tok_dn.at[row], tok_recv.at[row * 2 + b], jnp.maximum(e - 2, b), t)
-
-    def x_copy(row):
-        return token_copy(row * 2 + b, c, tok_x.at[row], tok_recv.at[row * 2 + b], a * 2 + 1 - b, t)
-
-    def sib_copy(blk):
-        return token_copy(blk, c, tok_sib.at[blk], tok_recv_sib.at[blk], e, sib)
-
-    def forward(row):
+    def line_copy(row, piece, sent, ep):
+        blk = row * 2 + b
+        return token_copy(blk, piece, c, sent.at[row, piece], tok_recv.at[blk, piece], ep, t)
+
+    def up_copy(row, piece):
+        return line_copy(row, piece, tok_up, jnp.minimum(e + 2, n_ep - 2 + b))
+
+    def dn_copy(row, piece):
+        return line_copy(row, piece, tok_dn, jnp.maximum(e - 2, b))
+
+    def x_copy(row, piece):
+        return line_copy(row, piece, tok_x, a * 2 + 1 - b)
+
+    def sib_copy(blk, piece):
+        return token_copy(blk, piece, c, tok_sib.at[blk, piece], tok_recv_sib.at[blk, piece], e, sib)
+
+    def forward(row, piece):
         @pl.when((row <= a) & (a + 1 < n_line))
         def _():
-            up_copy(row).start()
+            up_copy(row, piece).start()
 
         @pl.when((row >= a) & (a >= 1))
         def _():
-            dn_copy(row).start()
-
-        x_copy(row).start()
-
-    def hid_y_copy(s, yy):
-        part = hid.at[s, c, y]
+            dn_copy(row, piece).start()
+
+        x_copy(row, piece).start()
+
+    def piece_of(piece):
+        return pl.ds(piece * piece_rows, piece_rows)
+
+    def hid_y_copy(s, piece, yy):
+        part = hid.at[s, c, y, piece_of(piece)]
         return pltpu.make_async_remote_copy(
-            part, part, hid_send_y.at[s], hid_recv_y.at[s], device_id={"ep": e, "tp": yy * 2 + c}, device_id_type=MESH
-        )
-
-    def hid_sib_copy(s, yy):
-        part = hid.at[s, c, yy]
+            part, part, hid_send_y.at[s, piece], hid_recv_y.at[s, piece],
+            device_id={"ep": e, "tp": yy * 2 + c}, device_id_type=MESH,
+        )
+
+    def hid_sib_copy(s, piece, yy):
+        part = hid.at[s, c, yy, piece_of(piece)]
         return pltpu.make_async_remote_copy(
-            part, part, hid_send_sib.at[s], hid_recv_sib.at[s], device_id={"ep": e, "tp": sib}, device_id_type=MESH
+            part, part, hid_send_sib.at[s, piece], hid_recv_sib.at[s, piece],
+            device_id={"ep": e, "tp": sib}, device_id_type=MESH,
         )
 
     def span(ref, send, recv):
@@ -196,26 +209,39 @@
             ref, ref, send, recv, device_id={"ep": e, "tp": sib}, device_id_type=MESH
         )
 
-    def gated(rows, gate_w, up_w, s):
+    def from_y(s, piece):
+        ref = hid.at[s, c, pl.ds(0, n_y - 1), piece_of(piece)]
+        return span(ref, hid_send_y.at[s, piece], hid_recv_y.at[s, piece])
+
+    def from_sib(s, piece, core):
+        return span(hid.at[s, core, :, piece_of(piece)], hid_send_sib.at[s, piece], hid_recv_sib.at[s, piece])
+
+    def gated(rows, gate_w, up_w, targets):
         block = min(256, hidden)
         for n in range(hidden // block):
             cols = pl.ds(n * block, block)
             gate_part = dot(rows, gate_w[:, cols])
             up_part = dot(rows, up_w[:, cols])
-            hid[s, c, y, :, cols] = (gate_part / (1.0 + jnp.exp(-gate_part)) * up_part).astype(bf16)
-
-    def send_hidden(s):
+            value = (gate_part / (1.0 + jnp.exp(-gate_part)) * up_part).astype(bf16)
+            done = 0
+            for s, into in targets:
+                hid[s, c, y, into, cols] = value[done : done + into.size]
+                done += into.size
+
+    def send_hidden(s, piece):
         for dy in range(1, n_y):
-            hid_y_copy(s, lax.rem(y + dy, n_y)).start()
-        hid_sib_copy(s, y).start()
+            hid_y_copy(s, piece, lax.rem(y + dy, n_y)).start()
+        hid_sib_copy(s, piece, y).start()
 
     def relay_hidden(s):
-        span(hid.at[s, c, pl.ds(0, n_y - 1)], hid_send_y.at[s], hid_recv_y.at[s]).wait_recv()
-        for dy in range(1, n_y):
-            hid_sib_copy(s, lax.rem(y + dy, n_y)).start()
+        for piece in range(PIECES):
+            from_y(s, piece).wait_recv()
+            for dy in range(1, n_y):
+                hid_sib_copy(s, piece, lax.rem(y + dy, n_y)).start()
 
     def down_product(s, weight):
-        span(hid.at[s, 1 - c], hid_send_sib.at[s], hid_recv_sib.at[s]).wait_recv()
+        for piece in range(PIECES):
+            from_sib(s, piece, 1 - c).wait_recv()
         value = None
         for cc in range(2):
             for yy in range(n_y):
@@ -224,25 +250,46 @@
                 value = term if value is None else value + term
         return value
 
-    def res_copy(blk):
+    late_target = lax.rem(a + n_line // 2, n_line) * 2 + 1 - b
+    late_source = lax.rem(a + n_line - n_line // 2, n_line) * 2 + 1 - b
+
+    def res_copy(blk, into):
         return pltpu.make_async_remote_copy(
-            res.at[blk], ret.at[e], res_send.at[blk], res_recv.at[e], device_id={"ep": blk, "tp": t}, device_id_type=MESH
+            res.at[blk], into, res_send.at[blk], res_recv.at[e], device_id={"ep": blk, "tp": t}, device_id_type=MESH
+        )
+
+    def send_result(blk):
+        @pl.when(blk == late_target)
+        def _():
+            res_copy(blk, late_hbm).start()
+
+        @pl.when(blk != late_target)
+        def _():
+            res_copy(blk, ret.at[e]).start()
+
+    def from_expert(i, into):
+        return pltpu.make_async_remote_copy(
+            into, into, res_send.at[i], res_recv.at[i], device_id={"ep": e, "tp": sib}, device_id_type=MESH
         )
 
     loads[0].wait()
     loads[1].wait()
     tok[e] = scaled_rows(x[...], gain[...])
     pl.semaphore_wait(barrier, n_ep + n_tp - 2)
-    forward(a)
+    for piece in range(PIECES):
+        forward(a, piece)
 
     loads[2].wait()
     loads[3].wait()
-    gated(tok[e], sgate, sup, steps)
-    send_hidden(steps)
+    everything = pl.ds(0, token_rows)
+    gated(tok[e], sgate, sup, [(steps, everything)])
+    for piece in range(PIECES):
+        send_hidden(steps, piece)
     loads[4].wait()
     loads[5].wait()
-    gated(tok[e], gate, up, 0)
-    send_hidden(0)
+    gated(tok[e], gate, up, [(0, everything)])
+    for piece in range(PIECES):
+        send_hidden(0, piece)
 
     for k in range(6, 14):
         loads[k].wait()
@@ -297,28 +344,25 @@
             ai_ref[at, lanes] = reach[1]
             br_ref[at, lanes] = state[0]
             bi_ref[at, lanes] = state[1]
-        row = iota((ROWS, LANES), 0)
-        er, ei = jnp.ones((1, LANES), f32), jnp.zeros((1, LANES), f32)
-        sr, si = jnp.zeros((1, LANES), f32), jnp.zeros((1, LANES), f32)
-        pre_r = pre_i = pre_sr = pre_si = jnp.zeros((ROWS, LANES), f32)
+        for q, value in enumerate(reach + state):
+            for k in range(ROWS):
+                whole[q, k, pl.ds(i, 1), :] = value[k : k + 1]
+
+    def close_segments():
+        one_row, zero = jnp.ones((tiles, LANES), f32), jnp.zeros((tiles, LANES), f32)
+        er, ei, sr, si = one_row, zero, zero, zero
         for k in range(ROWS):
-            here = row == k
-            pre_r = jnp.where(here, er, pre_r)
-            pre_i = jnp.where(here, ei, pre_i)
-            pre_sr = jnp.where(here, sr, pre_sr)
-            pre_si = jnp.where(here, si, pre_si)
-            tr, ti = reach[0][k : k + 1], reach[1][k : k + 1]
-            ur, ui = state[0][k : k + 1], state[1][k : k + 1]
+            for q, value in enumerate((er, ei, sr, si)):
+                pre[q, k] = value
+            tr, ti, ur, ui = whole[0, k], whole[1, k], whole[2, k], whole[3, k]
             er, ei, sr, si = (
                 tr * er - ti * ei,
                 tr * ei + ti * er,
                 tr * sr - ti * si + ur,
                 tr * si + ti * sr + ui,
             )
-        for q, value in enumerate((pre_r, pre_i, pre_sr, pre_si)):
-            pre[q, i] = value
         for q, value in enumerate((er, ei, sr, si)):
-            ends[e, q, pl.ds(i, 1), :] = value
+            ends[e, q] = value
 
     def ends_copy(i):
         return pltpu.make_async_remote_copy(
@@ -326,6 +370,7 @@
         )
 
     def send_ends():
+        close_segments()
         for i in range(1, n_ep):
             @pl.when(i > e)
             def _():
@@ -354,7 +399,7 @@
     def read_tile(i):
         lanes = pl.ds(pl.multiple_of(i * LANES, LANES), LANES)
         ir, ii = inc[0, pl.ds(i, 1), :], inc[1, pl.ds(i, 1), :]
-        pre_r, pre_i, pre_sr, pre_si = pre[0, i], pre[1, i], pre[2, i], pre[3, i]
+        pre_r, pre_i, pre_sr, pre_si = (pre[q, :, pl.ds(i, 1), :].reshape(ROWS, LANES) for q in range(4))
         enter_r = (pre_sr + pre_r * ir - pre_i * ii)[None]
         enter_i = (pre_si + pre_r * ii + pre_i * ir)[None]
         shape = (segment, ROWS, LANES)
@@ -380,9 +425,16 @@
             part, part, ssm_sem.at[2], ssm_sem.at[3], device_id={"ep": e, "tp": sib}, device_id_type=MESH
         )
 
-    def read_out():
+    def read_tiles(first, last):
+        lax.fori_loop(first, last, lambda i, _: (read_tile(i), 0)[1], 0)
+
+    def begin_read():
+        incoming()
         total[...] = feed[...] * us[...].astype(f32)
-        lax.fori_loop(0, tiles, lambda i, _: (read_tile(i), 0)[1], 0)
+        read_tiles(0, tiles // 2)
+
+    def end_read():
+        read_tiles(tiles // 2, tiles)
         value = total[...]
         inner = 0.7978845608028654 * (value + 0.044715 * (value * value * value))
         result = (0.5 * value * (1.0 + jnp.tanh(inner))).astype(bf16)
@@ -395,26 +447,42 @@
     for k in range(14, 20):
         loads[k].wait()
 
-    early = min(EARLY_TILES, tiles)
-    lax.fori_loop(0, early, lambda i, _: (tile_work(i), 0)[1], 0)
-
-    def arrive(s):
-        row, other = place(s)
-        blk = block_of(row, other)
-        token_copy(blk, c, tok_sib.at[blk], tok_recv.at[blk], e, sib).wait_recv()
-
-        @pl.when(other == 0)
-        def _():
-            forward(row)
-
-        sib_copy(blk).start()
-
-    def first_products(s):
-        row, other = place(s)
-        blk = block_of(row, other)
-        token_copy(blk, 1 - c, tok_sib.at[blk], tok_recv_sib.at[blk], e, sib).wait_recv()
-        gated(tok[blk], gate, up, s)
-        send_hidden(s)
+    def tiles_between(first, last):
+        lax.fori_loop(jnp.minimum(first, tiles), jnp.minimum(last, tiles), lambda i, _: (tile_work(i), 0)[1], 0)
+
+    def arrive(s, piece):
+        @pl.when((s >= 0) & (s < steps))
+        def _():
+            row, other = place(s)
+            blk = block_of(row, other)
+            token_copy(blk, piece, c, tok_sib.at[blk, piece], tok_recv.at[blk, piece], e, sib).wait_recv()
+
+            @pl.when(other == 0)
+            def _():
+                forward(row, piece)
+
+            sib_copy(blk, piece).start()
+
+    def first_products(p, piece):
+        def whole_rows(s):
+            row, other = place(s)
+            blk = block_of(row, other)
+            token_copy(blk, piece, 1 - c, tok_sib.at[blk, piece], tok_recv_sib.at[blk, piece], e, sib).wait_recv()
+            return tok[blk, piece_of(piece)]
+
+        one_s, two_s = 2 * p - 1, 2 * p
+
+        @pl.when(two_s < steps)
+        def _():
+            rows = jnp.concatenate([whole_rows(one_s), whole_rows(two_s)], axis=0)
+            gated(rows, gate, up, [(one_s, piece_of(piece)), (two_s, piece_of(piece))])
+            send_hidden(one_s, piece)
+            send_hidden(two_s, piece)
+
+        @pl.when((one_s < steps) & (two_s >= steps))
+        def _():
+            gated(whole_rows(one_s), gate, up, [(one_s, piece_of(piece))])
+            send_hidden(one_s, piece)
 
     def held(s):
         return (s == 2) & (short < 1) & (steps >= 6)
@@ -434,73 +502,85 @@
 
         @pl.when((blk != e) & jnp.logical_not(held(s)))
         def _():
-            res_copy(blk).start()
-
-    last_pair = steps // 2
+            send_result(blk)
+
 
     def one(q, act):
         @pl.when((q >= 0) & (q < steps))
         def _():
             act(q)
 
+    arrive(1, 0)
+    arrive(2, 0)
+    tiles_between(0, 1)
+
     def pair(p, carry):
-        one(2 * p - 1, arrive)
-        one(2 * p, arrive)
+        first_products(p, 0)
+
+        @pl.when(p == 1)
+        def _():
+            tiles_between(1, 2)
+
+        for piece in range(1, PIECES):
+            arrive(2 * p - 1, piece)
+            arrive(2 * p, piece)
 
         @pl.when((p == 3) & (short < 1) & (steps >= 6))
         def _():
             row, other = place(2)
-            res_copy(block_of(row, other)).start()
-
-        one(2 * p - 1, first_products)
-
-        @pl.when(p != last_pair)
+            send_result(block_of(row, other))
+
+        @pl.when(p == 1)
+        def _():
+            tiles_between(2, 3)
+
+        @pl.when(p >= 2)
         def _():
             one(2 * p - 3, relay_hidden)
 
-        @pl.when(p == last_pair)
+        for piece in range(1, PIECES):
+            first_products(p, piece)
+
+        @pl.when(p == 5)
+        def _():
+            end_read()
+
+        @pl.when(p >= 2)
         def _():
             one(2 * p - 3, last_product)
-
-        one(2 * p, first_products)
-        one(2 * p - 2, relay_hidden)
+            one(2 * p - 2, relay_hidden)
+
+        arrive(2 * p + 1, 0)
+        arrive(2 * p + 2, 0)
 
         @pl.when(p == 1)
         def _():
             relay_hidden(steps)
-
-        @pl.when(p <= 2)
-        def _():
-            middle = (early + tiles) // 2
-            lax.fori_loop(jnp.where(p == 1, early, middle), jnp.where(p == 1, middle, tiles), lambda i, _: (tile_work(i), 0)[1], 0)
+            relay_hidden(0)
+            tiles_between(3, TILES_IN_FIRST)
 
         @pl.when(p == 2)
         def _():
+            tiles_between(TILES_IN_FIRST, tiles)
             send_ends()
 
-        @pl.when(p != last_pair)
-        def _():
-            one(2 * p - 3, last_product)
-
-        one(2 * p - 2, last_product)
-
-        @pl.when(p == last_pair - 1)
-        def _():
-            incoming()
-            read_out()
-            one(2 * p - 1, relay_hidden)
-
-        @pl.when(p == last_pair)
-        def _():
-            span(ssm.at[c, pl.ds(0, n_y - 1)], ssm_sem.at[0], ssm_sem.at[1]).wait_recv()
-            for dy in range(1, n_y):
-                ssm_sib_copy(lax.rem(y + dy, n_y)).start()
-            shared_cols[...] = down_product(steps, sdown)
+        @pl.when(p == 4)
+        def _():
+            begin_read()
+
+        @pl.when(p >= 2)
+        def _():
+            one(2 * p - 2, last_product)
 
         return carry
 
     lax.fori_loop(1, steps // 2 + 2, pair, 0)
-
+    last_product(0)
+    shared_cols[...] = down_product(steps, sdown)
+
+    span(ssm.at[c, pl.ds(0, n_y - 1)], ssm_sem.at[0], ssm_sem.at[1]).wait_recv()
+    for dy in range(1, n_y):
+        ssm_sib_copy(lax.rem(y + dy, n_y)).start()
     span(ssm.at[1 - c], ssm_sem.at[2], ssm_sem.at[3]).wait_recv()
     squares = jnp.zeros((positions, 1), f32)
     for cc in range(2):
@@ -530,31 +610,37 @@
         taken = taken + jnp.where(iota((n_ep, token_rows), 0) == routes[k : k + 1, :], chosen[k : k + 1, :], 0.0)
     shares[...] = taken.T
 
+    def share_of(i):
+        return jnp.sum(jnp.where(iota((token_rows, n_ep), 1) == i, shares[...], 0.0), axis=1, keepdims=True)
+
+    late_weight[...] = jnp.broadcast_to(share_of(late_source), late_weight.shape)
+    weight_store = pltpu.make_async_copy(late_weight, weight_hbm, store_sem.at[2])
+    weight_store.start()
+
     def combine(s, carry):
         row, other = place(s)
         i = block_of(row, other)
 
-        @pl.when(i != e)
-        def _():
-            part = ret.at[i]
-            pltpu.make_async_remote_copy(
-                part, part, res_send.at[i], res_recv.at[i], device_id={"ep": e, "tp": sib}, device_id_type=MESH
-            ).wait_recv()
-
-        share = jnp.sum(jnp.where(iota((token_rows, n_ep), 1) == i, shares[...], 0.0), axis=1, keepdims=True)
-        shared_cols[...] += ret[i].astype(f32) * share
+        @pl.when((i != e) & (i != late_source))
+        def _():
+            from_expert(i, ret.at[i]).wait_recv()
+
+        @pl.when(i != late_source)
+        def _():
+            shared_cols[...] += ret[i].astype(f32) * share_of(i)
+
         return carry
 
     lax.fori_loop(0, steps, combine, 0)
-    moe_ref[...] = shared_cols[...].astype(bf16)
-    moe_store = pltpu.make_async_copy(moe_ref, moe_hbm, store_sem.at[1])
-    moe_store.start()
+    sum_store = pltpu.make_async_copy(shared_cols, sum_hbm, store_sem.at[1])
+    sum_store.start()
 
     def drain(s, carry):
         @pl.when(s != e)
         def _():
-            token_copy(s, c, tok_sib.at[s], tok_recv_sib.at[s], e, sib).wait_send()
-            res_copy(s).wait_send()
+            for piece in range(PIECES):
+                sib_copy(s, piece).wait_send()
+            res_copy(s, ret.at[e]).wait_send()
 
         @pl.when(s > e)
         def _():
@@ -565,45 +651,51 @@
     lax.fori_loop(0, n_ep, drain, 0)
 
     def drain_line(row, carry):
-        @pl.when((row <= a) & (a + 1 < n_line))
-        def _():
-            up_copy(row).wait_send()
-
-        @pl.when((row >= a) & (a >= 1))
-        def _():
-            dn_copy(row).wait_send()
-
-        x_copy(row).wait_send()
+        for piece in range(PIECES):
+            @pl.when((row <= a) & (a + 1 < n_line))
+            def _():
+                up_copy(row, piece).wait_send()
+
+            @pl.when((row >= a) & (a >= 1))
+            def _():
+                dn_copy(row, piece).wait_send()
+
+            x_copy(row, piece).wait_send()
         return carry
 
     lax.fori_loop(0, n_line, drain_line, 0)
 
     def drain_hidden(s, carry):
-        span(hid.at[s, c, pl.ds(0, n_y - 1)], hid_send_y.at[s], hid_recv_y.at[s]).wait_send()
-        span(hid.at[s, c], hid_send_sib.at[s], hid_recv_sib.at[s]).wait_send()
+        for piece in range(PIECES):
+            from_y(s, piece).wait_send()
+            from_sib(s, piece, c).wait_send()
         return carry
 
     lax.fori_loop(0, steps + 1, drain_hidden, 0)
     span(ssm.at[c, pl.ds(0, n_y - 1)], ssm_sem.at[0], ssm_sem.at[1]).wait_send()
     span(ssm.at[c], ssm_sem.at[2], ssm_sem.at[3]).wait_send()
     mixed_store.wait()
-    moe_store.wait()
-
-
-def hand_over(mixed, moe_out):
-    def copy(mixed_in, moe_in, mixed_ref, moe_ref):
+    weight_store.wait()
+    sum_store.wait()
+    from_expert(late_source, late_hbm).wait_recv()
+
+
+def hand_over(mixed, sums, late, weight):
+    def finish(mixed_in, sum_in, late_in, weight_in, mixed_ref, moe_ref):
         mixed_ref[...] = mixed_in[...]
-        moe_ref[...] = moe_in[...]
-
-    specs = [pl.BlockSpec(v.shape, lambda i: (0, 0)) for v in (mixed, moe_out)]
+        moe_ref[...] = (sum_in[...] + late_in[...].astype(f32) * weight_in[:, 0:1]).astype(bf16)
+
+    def whole(v):
+        return pl.BlockSpec(v.shape, lambda i: (0, 0))
+
     return pl.pallas_call(
-        copy,
+        finish,
         grid=(1,),
-        in_specs=specs,
-        out_specs=specs,
-        out_shape=[jax.ShapeDtypeStruct(v.shape, v.dtype) for v in (mixed, moe_out)],
+        in_specs=[whole(v) for v in (mixed, sums, late, weight)],
+        out_specs=[whole(mixed), whole(late)],
+        out_shape=[jax.ShapeDtypeStruct(v.shape, v.dtype) for v in (mixed, late)],
         name="hand_over",
-    )(mixed, moe_out)
+    )(mixed, sums, late, weight)
 
 
 def on_device(*operands):
@@ -648,35 +740,39 @@
         pltpu.VMEM((2, channels, lanes_all), bf16),
         pltpu.VMEM((2, channels, lanes_all), bf16),
         wide, wide, wide, wide,
-        pltpu.VMEM((4, tiles, ROWS, LANES), f32),
+        pltpu.VMEM((4, ROWS, tiles, LANES), f32),
+        pltpu.VMEM((4, ROWS, tiles, LANES), f32),
         pltpu.VMEM((2, tiles, LANES), f32),
         pltpu.VMEM((positions, channels), f32),
         pltpu.VMEM((token_rows, columns), f32),
         pltpu.VMEM((token_rows, n_ep), f32),
         dma((len(given),)),
-        dma((n_ep // 2,)), dma((n_ep // 2,)), dma((n_ep // 2,)), dma((n_ep,)), dma((n_ep,)), dma((n_ep,)),
-        dma((n_ep + 1,)), dma((n_ep + 1,)), dma((n_ep + 1,)), dma((n_ep + 1,)),
+        dma((n_ep // 2, PIECES)), dma((n_ep // 2, PIECES)), dma((n_ep // 2, PIECES)),
+        dma((n_ep, PIECES)), dma((n_ep, PIECES)), dma((n_ep, PIECES)),
+        dma((n_ep + 1, PIECES)), dma((n_ep + 1, PIECES)), dma((n_ep + 1, PIECES)), dma((n_ep + 1, PIECES)),
         dma((n_ep,)), dma((n_ep,)), dma((n_ep,)), dma((n_ep,)),
         dma((4,)),
-        dma((2,)),
+        dma((3,)),
         pltpu.VMEM((positions, columns), bf16),
-        pltpu.VMEM((token_rows, columns), bf16),
+        pltpu.VMEM((token_rows, LANES), f32),
     ]
-    mixed, moe_out = pl.pallas_call(
+    parts_out = pl.pallas_call(
         functools.partial(body, n_ep, n_tp),
         out_shape=[
             jax.ShapeDtypeStruct((positions, columns), bf16),
+            jax.ShapeDtypeStruct((token_rows, columns), f32),
             jax.ShapeDtypeStruct((token_rows, columns), bf16),
+            jax.ShapeDtypeStruct((token_rows, LANES), f32),
         ],
         in_specs=[pl.BlockSpec(memory_space=pl.ANY)] * len(given),
-        out_specs=[pl.BlockSpec(memory_space=pl.ANY)] * 2,
+        out_specs=[pl.BlockSpec(memory_space=pl.ANY)] * 4,
         scratch_shapes=scratch,
         compiler_params=pltpu.CompilerParams(
             collective_id=0, has_side_effects=True, vmem_limit_bytes=VMEM_BYTES
         ),
         name="both_batches",
     )(*given)
-    return hand_over(mixed, moe_out)
+    return hand_over(*parts_out)
 
 
 def solution(mesh):

time: 56.7 us -> 54.6 us (0.963)
  Pallas kernels: 55.9 us -> 53.8 us
    pallas_call x1, Pallas kernels: 54.2 us -> 52 us  [on_device(): pl.pallas_call(functools.partial(body, n_ep, n_tp), out_shape=[jax.ShapeD...]
where the time goes in v3:
time: 54.6 us; the launch traced here: 54.5 us
  Pallas kernels  53.8 us (99%)
  between operations  0.65 us (1%)
    pallas_call x1, Pallas kernels, on_device(): pl.pallas_call(functools.partial(body, n_ep, n_tp), out_shape=[jax.ShapeD...  52 us
    pallas_call x1, Pallas kernels, hand_over(): pl.pallas_call(finish, grid=(1,), in_specs=[whole(v) for v in (mixed, sum...  1.83 us

profile of v3, /device:TPU:0, one launch (start us, length us, event | category | flops | bytes accessed | tf_op | source)
XLA Modules:
  0.0 54.5 jit_solution(10572084160120085717)
XLA Ops:
  0.6 52.0 %both_batches.1 = (bf16[256,512]{1,0:T(8,128)(2,1)}, f32[128,512]{1,0:T(8,128)}, bf16[128,512]{1,0:T(8,128)(2,1)}, f32[128,128]{1,0:T(8,128)}) custom-call(bf16[256,256]{1,0:T(8,128)(2,1)} %u_hbm.1, f32[16,256]{1,0:T(8,128)} %logs_hbm.1, f32[16,256]{1,0:T(8,128)} %loss_hbm.1, f32[16,64]{1,0:T(8,128)} %eig_hbm.1, f32[16,64]{1,0:T(8,128)} %freq_hbm.1, ...), custom_call_target="tpu_custom_call" | custom-call | tf_op jit(solution)/shard_map/both_batches/pallas_call | solution.py:759
  52.6 1.8 %hand_over.1 = (bf16[256,512]{1,0:T(8,128)(2,1)}, bf16[128,512]{1,0:T(8,128)(2,1)}) custom-call(bf16[256,512]{1,0:T(8,128)(2,1)} %get-tuple-element.6.mixed_in, f32[128,512]{1,0:T(8,128)} %get-tuple-element.7.sum_in, bf16[128,512]{1,0:T(8,128)(2,1)} %get-tuple-element.8.late_in, f32[128,128]{1,0:T(8,128)} %get-tuple-element.9.weight_in), custom_call_target="tpu_custom_call" | custom-call | tf_op jit(solution)/shard_map/hand_over/pallas_call | solution.py:691

commit v4 on v3

--- a/solution.py
+++ b/solution.py
@@ -82,7 +82,7 @@
     load_sem,
     tok_up, tok_dn, tok_x, tok_sib, tok_recv, tok_recv_sib,
     hid_send_y, hid_send_sib, hid_recv_y, hid_recv_sib,
-    res_send, res_recv, ends_send, ends_recv,
+    res_send, res_recv, ends_sem,
     ssm_sem, store_sem, mixed_ref, late_weight,
 ):
     e, t = lax.axis_index("ep"), lax.axis_index("tp")
@@ -162,19 +162,19 @@
 
     def line_copy(row, piece, sent, ep):
         blk = row * 2 + b
-        return token_copy(blk, piece, c, sent.at[row, piece], tok_recv.at[blk, piece], ep, t)
+        return token_copy(blk, piece, c, sent, tok_recv.at[blk, piece], ep, t)
 
     def up_copy(row, piece):
-        return line_copy(row, piece, tok_up, jnp.minimum(e + 2, n_ep - 2 + b))
+        return line_copy(row, piece, tok_up.at[row, piece], jnp.minimum(e + 2, n_ep - 2 + b))
 
     def dn_copy(row, piece):
-        return line_copy(row, piece, tok_dn, jnp.maximum(e - 2, b))
+        return line_copy(row, piece, tok_dn.at[row, piece], jnp.maximum(e - 2, b))
 
     def x_copy(row, piece):
-        return line_copy(row, piece, tok_x, a * 2 + 1 - b)
+        return line_copy(row, piece, tok_x.at[0], a * 2 + 1 - b)
 
     def sib_copy(blk, piece):
-        return token_copy(blk, piece, c, tok_sib.at[blk, piece], tok_recv_sib.at[blk, piece], e, sib)
+        return token_copy(blk, piece, c, tok_sib.at[0], tok_recv_sib.at[blk, piece], e, sib)
 
     def forward(row, piece):
         @pl.when((row <= a) & (a + 1 < n_line))
@@ -184,8 +184,6 @@
         @pl.when((row >= a) & (a >= 1))
         def _():
             dn_copy(row, piece).start()
-
-        x_copy(row, piece).start()
 
     def piece_of(piece):
         return pl.ds(piece * piece_rows, piece_rows)
@@ -193,14 +191,14 @@
     def hid_y_copy(s, piece, yy):
         part = hid.at[s, c, y, piece_of(piece)]
         return pltpu.make_async_remote_copy(
-            part, part, hid_send_y.at[s, piece], hid_recv_y.at[s, piece],
+            part, part, hid_send_y.at[0], hid_recv_y.at[s],
             device_id={"ep": e, "tp": yy * 2 + c}, device_id_type=MESH,
         )
 
     def hid_sib_copy(s, piece, yy):
         part = hid.at[s, c, yy, piece_of(piece)]
         return pltpu.make_async_remote_copy(
-            part, part, hid_send_sib.at[s, piece], hid_recv_sib.at[s, piece],
+            part, part, hid_send_sib.at[0], hid_recv_sib.at[s],
             device_id={"ep": e, "tp": sib}, device_id_type=MESH,
         )
 
@@ -209,12 +207,11 @@
             ref, ref, send, recv, device_id={"ep": e, "tp": sib}, device_id_type=MESH
         )
 
-    def from_y(s, piece):
-        ref = hid.at[s, c, pl.ds(0, n_y - 1), piece_of(piece)]
-        return span(ref, hid_send_y.at[s, piece], hid_recv_y.at[s, piece])
-
-    def from_sib(s, piece, core):
-        return span(hid.at[s, core, :, piece_of(piece)], hid_send_sib.at[s, piece], hid_recv_sib.at[s, piece])
+    def from_y(s):
+        return span(hid.at[s, c, pl.ds(0, n_y - 1)], hid_send_y.at[0], hid_recv_y.at[s])
+
+    def from_sib(s):
+        return span(hid.at[s, 1 - c], hid_send_sib.at[0], hid_recv_sib.at[s])
 
     def gated(rows, gate_w, up_w, targets):
         block = min(256, hidden)
@@ -234,14 +231,13 @@
         hid_sib_copy(s, piece, y).start()
 
     def relay_hidden(s):
-        for piece in range(PIECES):
-            from_y(s, piece).wait_recv()
-            for dy in range(1, n_y):
-                hid_sib_copy(s, piece, lax.rem(y + dy, n_y)).start()
+        from_y(s).wait_recv()
+        for dy in range(1, n_y):
+            part = hid.at[s, c, lax.rem(y + dy, n_y)]
+            span(part, hid_send_sib.at[0], hid_recv_sib.at[s]).start()
 
     def down_product(s, weight):
-        for piece in range(PIECES):
-            from_sib(s, piece, 1 - c).wait_recv()
+        from_sib(s).wait_recv()
         value = None
         for cc in range(2):
             for yy in range(n_y):
@@ -255,7 +251,7 @@
 
     def res_copy(blk, into):
         return pltpu.make_async_remote_copy(
-            res.at[blk], into, res_send.at[blk], res_recv.at[e], device_id={"ep": blk, "tp": t}, device_id_type=MESH
+            res.at[blk], into, res_send.at[0], res_recv.at[e], device_id={"ep": blk, "tp": t}, device_id_type=MESH
         )
 
     def send_result(blk):
@@ -269,7 +265,7 @@
 
     def from_expert(i, into):
         return pltpu.make_async_remote_copy(
-            into, into, res_send.at[i], res_recv.at[i], device_id={"ep": e, "tp": sib}, device_id_type=MESH
+            into, into, res_send.at[0], res_recv.at[i], device_id={"ep": e, "tp": sib}, device_id_type=MESH
         )
 
     loads[0].wait()
@@ -278,6 +274,7 @@
     pl.semaphore_wait(barrier, n_ep + n_tp - 2)
     for piece in range(PIECES):
         forward(a, piece)
+        x_copy(a, piece).start()
 
     loads[2].wait()
     loads[3].wait()
@@ -366,27 +363,27 @@
 
     def ends_copy(i):
         return pltpu.make_async_remote_copy(
-            ends.at[e], ends.at[e], ends_send.at[i], ends_recv.at[e], device_id={"ep": i, "tp": t}, device_id_type=MESH
+            ends.at[e], ends.at[e], ends_sem.at[0], ends_sem.at[1], device_id={"ep": i, "tp": t}, device_id_type=MESH
         )
 
     def send_ends():
         close_segments()
-        for i in range(1, n_ep):
-            @pl.when(i > e)
+        for i in range(n_ep):
+            @pl.when(i != e)
             def _():
                 ends_copy(i).start()
+
+    def all_ends():
+        return span(ends.at[pl.ds(0, n_ep - 1)], ends_sem.at[0], ends_sem.at[1])
 
     def incoming():
         zero = jnp.zeros((tiles, LANES), f32)
         inc[0] = zero
         inc[1] = zero
+        all_ends().wait_recv()
         for i in range(n_ep - 1):
             @pl.when(i < e)
             def _():
-                part = ends.at[i]
-                pltpu.make_async_remote_copy(
-                    part, part, ends_send.at[i], ends_recv.at[i], device_id={"ep": e, "tp": sib}, device_id_type=MESH
-                ).wait_recv()
                 tr, ti, ur, ui = ends[i, 0], ends[i, 1], ends[i, 2], ends[i, 3]
                 sr, si = inc[0], inc[1]
                 inc[0] = tr * sr - ti * si + ur
@@ -455,11 +452,23 @@
         def _():
             row, other = place(s)
             blk = block_of(row, other)
-            token_copy(blk, piece, c, tok_sib.at[blk, piece], tok_recv.at[blk, piece], e, sib).wait_recv()
+            token_copy(blk, piece, c, tok_sib.at[0], tok_recv.at[blk, piece], e, sib).wait_recv()
+
+            later = (s == 2) & (short >= 1)
 
             @pl.when(other == 0)
             def _():
                 forward(row, piece)
+
+            if piece == PIECES - 1:
+                @pl.when((other == 0) & later)
+                def _():
+                    for early in range(PIECES - 1):
+                        x_copy(row, early).start()
+
+            @pl.when((other == 0) & (jnp.logical_not(later) | (piece == PIECES - 1)))
+            def _():
+                x_copy(row, piece).start()
 
             sib_copy(blk, piece).start()
 
@@ -467,7 +476,7 @@
         def whole_rows(s):
             row, other = place(s)
             blk = block_of(row, other)
-            token_copy(blk, piece, 1 - c, tok_sib.at[blk, piece], tok_recv_sib.at[blk, piece], e, sib).wait_recv()
+            token_copy(blk, piece, 1 - c, tok_sib.at[0], tok_recv_sib.at[blk, piece], e, sib).wait_recv()
             return tok[blk, piece_of(piece)]
 
         one_s, two_s = 2 * p - 1, 2 * p
@@ -521,6 +530,10 @@
         def _():
             tiles_between(1, 2)
 
+        @pl.when(p == 3)
+        def _():
+            one(2 * p - 3, relay_hidden)
+
         for piece in range(1, PIECES):
             arrive(2 * p - 1, piece)
             arrive(2 * p, piece)
@@ -534,20 +547,36 @@
         def _():
             tiles_between(2, 3)
 
-        @pl.when(p >= 2)
+        @pl.when(p == 2)
         def _():
             one(2 * p - 3, relay_hidden)
+
+        @pl.when(p == 3)
+        def _():
+            one(2 * p - 3, last_product)
 
         for piece in range(1, PIECES):
             first_products(p, piece)
 
+        @pl.when(p >= 4)
+        def _():
+            one(2 * p - 3, relay_hidden)
+
         @pl.when(p == 5)
         def _():
             end_read()
 
-        @pl.when(p >= 2)
-        def _():
+        @pl.when(p >= 4)
+        def _():
+            one(2 * p - 2, relay_hidden)
             one(2 * p - 3, last_product)
+
+        @pl.when(p == 2)
+        def _():
+            one(2 * p - 3, last_product)
+
+        @pl.when((p == 2) | (p == 3))
+        def _():
             one(2 * p - 2, relay_hidden)
 
         arrive(2 * p + 1, 0)
@@ -635,20 +664,11 @@
     sum_store = pltpu.make_async_copy(shared_cols, sum_hbm, store_sem.at[1])
     sum_store.start()
 
-    def drain(s, carry):
-        @pl.when(s != e)
-        def _():
-            for piece in range(PIECES):
-                sib_copy(s, piece).wait_send()
-            res_copy(s, ret.at[e]).wait_send()
-
-        @pl.when(s > e)
-        def _():
-            ends_copy(s).wait_send()
-
-        return carry
-
-    lax.fori_loop(0, n_ep, drain, 0)
+    own_half = pl.ds(pl.multiple_of(c * half, half), half)
+    span(tok.at[pl.ds(0, n_ep - 1), :, own_half], tok_sib.at[0], tok_recv.at[0, 0]).wait_send()
+    span(tok.at[pl.ds(0, n_line), :, own_half], tok_x.at[0], tok_recv.at[0, 0]).wait_send()
+    span(res.at[pl.ds(0, n_ep - 1)], res_send.at[0], res_recv.at[0]).wait_send()
+    all_ends().wait_send()
 
     def drain_line(row, carry):
         for piece in range(PIECES):
@@ -660,18 +680,12 @@
             def _():
                 dn_copy(row, piece).wait_send()
 
-            x_copy(row, piece).wait_send()
         return carry
 
     lax.fori_loop(0, n_line, drain_line, 0)
 
-    def drain_hidden(s, carry):
-        for piece in range(PIECES):
-            from_y(s, piece).wait_send()
-            from_sib(s, piece, c).wait_send()
-        return carry
-
-    lax.fori_loop(0, steps + 1, drain_hidden, 0)
+    span(hid.at[:, c, pl.ds(0, n_y - 1)], hid_send_y.at[0], hid_recv_y.at[0]).wait_send()
+    span(hid.at[:, c], hid_send_sib.at[0], hid_recv_sib.at[0]).wait_send()
     span(ssm.at[c, pl.ds(0, n_y - 1)], ssm_sem.at[0], ssm_sem.at[1]).wait_send()
     span(ssm.at[c], ssm_sem.at[2], ssm_sem.at[3]).wait_send()
     mixed_store.wait()
@@ -747,10 +761,10 @@
         pltpu.VMEM((token_rows, columns), f32),
         pltpu.VMEM((token_rows, n_ep), f32),
         dma((len(given),)),
-        dma((n_ep // 2, PIECES)), dma((n_ep // 2, PIECES)), dma((n_ep // 2, PIECES)),
-        dma((n_ep, PIECES)), dma((n_ep, PIECES)), dma((n_ep, PIECES)),
-        dma((n_ep + 1, PIECES)), dma((n_ep + 1, PIECES)), dma((n_ep + 1, PIECES)), dma((n_ep + 1, PIECES)),
-        dma((n_ep,)), dma((n_ep,)), dma((n_ep,)), dma((n_ep,)),
+        dma((n_ep // 2, PIECES)), dma((n_ep // 2, PIECES)), dma((1,)),
+        dma((1,)), dma((n_ep, PIECES)), dma((n_ep, PIECES)),
+        dma((1,)), dma((1,)), dma((n_ep + 1,)), dma((n_ep + 1,)),
+        dma((1,)), dma((n_ep,)), dma((2,)),
         dma((4,)),
         dma((3,)),
         pltpu.VMEM((positions, columns), bf16),

time: 54.6 us -> 53.6 us (0.982)
  Pallas kernels: 53.8 us -> 52.8 us
    pallas_call x1, Pallas kernels: 52 us -> 51 us  [on_device(): pl.pallas_call(functools.partial(body, n_ep, n_tp), out_shape=[jax.ShapeD...]
where the time goes in v4:
time: 53.6 us; the launch traced here: 53.4 us
  Pallas kernels  52.8 us (99%)
  between operations  0.65 us (1%)
    pallas_call x1, Pallas kernels, on_device(): pl.pallas_call(functools.partial(body, n_ep, n_tp), out_shape=[jax.ShapeD...  51 us
    pallas_call x1, Pallas kernels, hand_over(): pl.pallas_call(finish, grid=(1,), in_specs=[whole(v) for v in (mixed, sum...  1.83 us

profile of v4, /device:TPU:0, one launch (start us, length us, event | category | flops | bytes accessed | tf_op | source)
XLA Modules:
  0.0 53.4 jit_solution(10684292665538308650)
XLA Ops:
  0.6 51.0 %both_batches.1 = (bf16[256,512]{1,0:T(8,128)(2,1)}, f32[128,512]{1,0:T(8,128)}, bf16[128,512]{1,0:T(8,128)(2,1)}, f32[128,128]{1,0:T(8,128)}) custom-call(bf16[256,256]{1,0:T(8,128)(2,1)} %u_hbm.1, f32[16,256]{1,0:T(8,128)} %logs_hbm.1, f32[16,256]{1,0:T(8,128)} %loss_hbm.1, f32[16,64]{1,0:T(8,128)} %eig_hbm.1, f32[16,64]{1,0:T(8,128)} %freq_hbm.1, ...), custom_call_target="tpu_custom_call" | custom-call | tf_op jit(solution)/shard_map/both_batches/pallas_call | solution.py:773
  51.6 1.8 %hand_over.1 = (bf16[256,512]{1,0:T(8,128)(2,1)}, bf16[128,512]{1,0:T(8,128)(2,1)}) custom-call(bf16[256,512]{1,0:T(8,128)(2,1)} %get-tuple-element.6.mixed_in, f32[128,512]{1,0:T(8,128)} %get-tuple-element.7.sum_in, bf16[128,512]{1,0:T(8,128)(2,1)} %get-tuple-element.8.late_in, f32[128,128]{1,0:T(8,128)} %get-tuple-element.9.weight_in), custom_call_target="tpu_custom_call" | custom-call | tf_op jit(solution)/shard_map/hand_over/pallas_call | solution.py:705
